TPU v7x, 128 devices: a whole 4x4x4 slice. The times are simulated.
128 devices in a mesh: fs: 16 (over z, y), tp: 8 (over x, core).
Axes of the slice: x: 4, y: 4, z: 4, core: 2. Of those that a mesh axis runs over, the one named last changes fastest.
Arguments:
- late_input: bfloat16 [8192, 2048], P(('fs', 'tp')), may hold values from -6 to 6
- early_input: bfloat16 [8192, 2048], P(('fs', 'tp')), may hold values from -6 to 6
- early_grad: bfloat16 [8192, 2048], P(('fs', 'tp')), may hold values from -24 to 24
- pre_gain: float32 [2048], replicated, may hold values from 0.1 to 1.9
- post_gain: float32 [2048], replicated, may hold values from 0.1 to 1.9
- gate_weight: bfloat16 [2048, 4096], P('fs', 'tp'), may hold values from -0.125 to 0.125
- up_weight: bfloat16 [2048, 4096], P('fs', 'tp'), may hold values from -0.125 to 0.125
- down_weight: bfloat16 [2048, 4096], P('fs', 'tp'), may hold values from -0.09375 to 0.09375
- gate_sum: float32 [2048, 4096], P('fs', 'tp'), may hold values from -1.8 to 1.8
- up_sum: float32 [2048, 4096], P('fs', 'tp'), may hold values from -1.8 to 1.8
- down_gradient_sum: float32 [2048, 4096], P('fs', 'tp'), may hold values from -1.8 to 1.8
Outputs:
- late_output: bfloat16 [8192, 2048], P(('fs', 'tp'))
- early_input_grad: bfloat16 [8192, 2048], P(('fs', 'tp'))
- gate_total: float32 [2048, 4096], P('fs', 'tp')
- up_total: float32 [2048, 4096], P('fs', 'tp')
- down_total: float32 [2048, 4096], P('fs', 'tp')
All inputs are finite; a program needn't handle non-finite values.
Results may differ from a plain program's by a relative error of at most 0.013.
Values may be sent and summed in bfloat16 or wider, within the bound.
A program may use at most 128 MiB of HBM per device.

v0:
```python
import math

import jax
import jax.numpy as jnp
from jax import lax
from jax.sharding import PartitionSpec as P

NORM_EPS = 1e-06


def sent_together(arrays, axis, dim, along):
    ends, at = ([], 0)
    for a in arrays[:-1]:
        at += a.shape[along]
        ends.append(at)
    both = jnp.concatenate(arrays, axis=along)
    return tuple(jnp.split(lax.all_gather(both, axis, axis=dim, tiled=True), ends, axis=along))


def sent_to_all(shard, axis):
    peers = lax.axis_size(axis)
    return lax.all_to_all(
        jnp.broadcast_to(shard[None], (peers, *shard.shape)), axis, 0, 0, tiled=True
    )


def in_order(parts, dim):
    parts = jnp.moveaxis(parts, 0, dim)
    dims = parts.shape
    return parts.reshape(*dims[:dim], dims[dim] * dims[dim + 1], *dims[dim + 2 :])


def gather_directly(shard, axis, dim):
    parts = sent_to_all(shard, axis)
    return in_order(parts, dim)


def in_blocks(shard, dim, peers):
    dims = shard.shape
    parts = shard.reshape(*dims[:dim], peers, dims[dim] // peers, *dims[dim + 1 :])
    return jnp.moveaxis(parts, dim, 0)


def summed_on_arrival(shard, axis, dim):
    parts = in_blocks(shard, dim, lax.axis_size(axis))
    arrived = lax.all_to_all(parts, axis, split_axis=0, concat_axis=0, tiled=True)
    return arrived.astype(jnp.float32).sum(axis=0)


def contract_last(first_op, second_op):
    return lax.dot_general(
        first_op, second_op, (((1,), (1,)), ((), ())), preferred_element_type=jnp.float32
    )


def contract_first(first_op, second_op):
    return lax.dot_general(
        first_op, second_op, (((0,), (0,)), ((), ())), preferred_element_type=jnp.float32
    )


def inverse_rms(values):
    return lax.rsqrt(jnp.mean(values * values, axis=-1, keepdims=True) + NORM_EPS)


def per_device(
    late_input,
    early_input,
    early_grad,
    pre_gain,
    post_gain,
    gate_weight,
    up_weight,
    down_weight,
    gate_sum,
    up_sum,
    down_gradient_sum,
):
    tok_rows, model_width = late_input.shape
    group_rows = tok_rows * lax.axis_size("tp")
    grad_scale = 1.0 / math.sqrt(group_rows * lax.axis_size("fs"))
    hidden_width = gate_sum.shape[1]
    input_rows = jnp.stack([late_input, early_input]).astype(jnp.float32)
    input_inverse = inverse_rms(input_rows)
    normed = (input_rows * input_inverse * pre_gain).astype(jnp.bfloat16)
    normed_rows = lax.all_gather(normed, "tp", axis=1, tiled=True)
    gate_all, up_all, down_gradient_rows = sent_together(
        (gate_weight, up_weight, down_weight), "fs", 0, 1
    )
    flat_rows = normed_rows.reshape(2 * group_rows, model_width)
    gate_pre = jnp.dot(flat_rows, gate_all, preferred_element_type=jnp.float32)
    up_pre = jnp.dot(flat_rows, up_all, preferred_element_type=jnp.float32)
    hidden_state = (
        (jax.nn.silu(gate_pre) * up_pre).astype(jnp.bfloat16).reshape(2, group_rows, hidden_width)
    )
    gated_product = jnp.einsum(
        "utx,ix->tui", hidden_state, down_gradient_rows, preferred_element_type=jnp.float32
    )
    mixed_sum = lax.psum_scatter(
        gated_product.reshape(lax.axis_size("tp") * tok_rows, 2 * model_width).astype(jnp.bfloat16),
        "tp",
        scatter_dimension=0,
        tiled=True,
    ).astype(jnp.float32)
    mixed_sum = lax.optimization_barrier(mixed_sum.astype(jnp.bfloat16)).astype(jnp.float32)
    mixed_sum = mixed_sum.reshape(tok_rows, 2, model_width)
    mixed_inverse = inverse_rms(mixed_sum)
    late_output = (input_rows[0] + 0.5 * mixed_sum[:, 0] * mixed_inverse[:, 0] * post_gain).astype(
        jnp.bfloat16
    )
    early_mixed = mixed_sum[:, 1]
    early_inverse_norm = mixed_inverse[:, 1]
    weighted = 0.5 * early_grad.astype(jnp.float32) * post_gain
    mixed_cot = (
        early_inverse_norm * weighted
        - early_mixed
        * early_inverse_norm**3
        * jnp.mean(weighted * early_mixed, axis=-1, keepdims=True)
    ).astype(jnp.bfloat16)
    cot_rows = gather_directly(mixed_cot, "tp", 0)
    early_hidden = hidden_state[1]
    early_normed = normed_rows[1]
    hidden_cot = jnp.dot(cot_rows, down_gradient_rows, preferred_element_type=jnp.float32)
    early_gate = gate_pre[group_rows:]
    early_up = up_pre[group_rows:]
    sigmoid_gate = jax.nn.sigmoid(early_gate)
    gate_cot = (
        hidden_cot * early_up * sigmoid_gate * (1.0 + early_gate * (1.0 - sigmoid_gate))
    ).astype(jnp.bfloat16)
    up_cot = (hidden_cot * early_gate * sigmoid_gate).astype(jnp.bfloat16)
    normed_cot = summed_on_arrival(
        (contract_last(gate_cot, gate_all) + contract_last(up_cot, up_all)).astype(jnp.bfloat16),
        "tp",
        0,
    )
    normed_cot = lax.optimization_barrier(normed_cot.astype(jnp.bfloat16)).astype(jnp.float32)
    weighted_in = normed_cot * pre_gain
    early_values = input_rows[1]
    early_in_inverse = input_inverse[1]
    early_input_grad = (
        early_grad.astype(jnp.float32)
        + early_in_inverse * weighted_in
        - early_values
        * early_in_inverse**3
        * jnp.mean(weighted_in * early_values, axis=-1, keepdims=True)
    ).astype(jnp.bfloat16)
    totals = lax.psum_scatter(
        (
            grad_scale
            * jnp.concatenate(
                [
                    contract_first(early_normed, gate_cot),
                    contract_first(early_normed, up_cot),
                    contract_first(cot_rows, early_hidden),
                ],
                1,
            )
        ).astype(jnp.bfloat16),
        "fs",
        scatter_dimension=0,
        tiled=True,
    ).astype(jnp.float32)
    gate_total = gate_sum + totals[:, :hidden_width]
    up_total = up_sum + totals[:, hidden_width : 2 * hidden_width]
    down_total = down_gradient_sum + totals[:, 2 * hidden_width :]
    return (late_output, early_input_grad, gate_total, up_total, down_total)


def solution(mesh):
    in_specs = (
        P(("fs", "tp"), None),
        P(("fs", "tp"), None),
        P(("fs", "tp"), None),
        P(),
        P(),
        P("fs", "tp"),
        P("fs", "tp"),
        P("fs", "tp"),
        P("fs", "tp"),
        P("fs", "tp"),
        P("fs", "tp"),
    )
    out_specs = (
        P(("fs", "tp"), None),
        P(("fs", "tp"), None),
        P("fs", "tp"),
        P("fs", "tp"),
        P("fs", "tp"),
    )
    return jax.shard_map(
        per_device, mesh=mesh, in_specs=in_specs, out_specs=out_specs, check_vma=False
    )
```

profile of v0, /device:TPU:0, one launch (start us, length us, event | category | flops | bytes accessed | tf_op | source)
XLA Modules:
  0.0 314.3 jit_solution(15130578604359886631)
XLA Ops:
  8.4 2.0 multiply_convert_fusion.2
  10.5 1.8 pad_maximum_fusion
  12.4 32.7 %all-gather.5.cloned.1.call-done = bf16[2,512,2048]{2,1,0:T(8,128)(2,1)} async-done(((bf16[2,64,2048]{2,1,0:T(8,128)(2,1)}), bf16[2,512,2048]{2,1,0:T(8,128)(2,1)}) %all-gather.5.cloned.1.call-update) | async-done | bytes 4194320 | tf_op jit(solution)/shard_map/all_gather | solution.py:86
  45.2 63.5 %all-gather.3.cloned.1.call-done = bf16[2048,1536]{1,0:T(8,128)(2,1)} async-done(((bf16[128,1536]{1,0:T(8,128)(2,1)}), bf16[2048,1536]{1,0:T(8,128)(2,1)}) %all-gather.3.cloned.1.call-update) | async-done | bytes 6291472 | tf_op jit(solution)/shard_map/all_gather | solution.py:17
  108.7 5.3 %fusion.9 = f32[1024,512]{1,0:T(8,128)S(1)} fusion(bf16[1024,2048]{1,0:T(8,128)(2,1)} %bitcast.66, bf16[2048,1536]{1,0:T(8,128)(2,1)} %all-gather.3.cloned.1.call-done), kind=kOutput, calls=%fused_computation.14 | convolution fusion | flops 2147483648 | bytes 8388608 | tf_op jit(solution)/shard_map/dot_general | solution.py:91
  114.6 3.9 %multiply_convert_fusion = (bf16[1024,512]{1,0:T(8,128)(2,1)S(1)}, f32[1024,512]{1,0:T(8,128)}) fusion(f32[1024,512]{1,0:T(8,128)S(1)} %fusion.9, bf16[1024,2048]{1,0:T(8,128)(2,1)S(1)} %bitcast.67, bf16[2048,1536]{1,0:T(8,128)(2,1)S(1)} %copy-done.2), kind=kOutput, calls=%fused_computation.6 | convolution fusion | flops 2150629376 | bytes 11534336 | tf_op jit(solution)/shard_map/dot_general | solution.py:92
  118.5 4.4 %convolution_convert_fusion = bf16[2048,2,512]{2,0,1:T(8,128)(2,1)} fusion(bf16[2,512,512]{2,1,0:T(8,128)(2,1)S(1)} %bitcast.75, bf16[2048,1536]{1,0:T(8,128)(2,1)S(1)} %copy-done.2), kind=kOutput, calls=%fused_computation.3 | convolution fusion | flops 2149580800 | bytes 7340032 | tf_op jit(solution)/shard_map/utx,ix->tui/dot_general | solution.py:96
  122.9 6.3 %copy.39 = bf16[512,4096]{1,0:T(8,128)(2,1)} copy(bf16[512,4096]{0,1:T(8,128)(2,1)} %bitcast.68) | data formatting | bytes 8388608 | tf_op jit(solution)/shard_map/convert_element_type | solution.py:100
  129.9 36.9 %reduce-scatter.5.cloned.1.call-done = bf16[64,4096]{1,0:T(8,128)(2,1)} async-done(((bf16[512,4096]{1,0:T(8,128)(2,1)}), bf16[64,4096]{1,0:T(8,128)(2,1)}) %reduce-scatter.5.cloned.1.call-update) | async-done | bytes 524304 | tf_op jit(solution)/shard_map/reduce_scatter | solution.py:99
  166.9 2.1 reshape.128
  168.9 1.6 fusion.31
  172.0 29.7 %all_to_all.10 = bf16[8,64,2048]{2,1,0:T(8,128)(2,1)S(1)} all-to-all(bf16[8,64,2048]{2,1,0:T(8,128)(2,1)S(1)} %broadcast_in_dim.2), channel_id=1, replica_groups=mesh['fs'=16,'tp'=8] {'tp'}, dimensions={0} | all-to-all | bytes 4194304 | tf_op jit(solution)/shard_map/all_to_all | solution.py:22
  201.6 1.3 fusion.24
  203.8 3.3 %multiply_convert_fusion.1 = (bf16[512,512]{1,0:T(8,128)(2,1)S(1)}, bf16[512,512]{1,0:T(8,128)(2,1)S(1)}) fusion(f32[1024,512]{1,0:T(8,128)S(1)} %copy-done.13, f32[1024,512]{1,0:T(8,128)S(1)} %copy-done.14, bf16[512,2048]{1,0:T(8,128)(2,1)S(1)} %bitcast.65, bf16[2048,1536]{1,0:T(8,128)(2,1)} %all-gather.3.cloned.1.call-done), kind=kOutput, calls=%fused_computation.23 | convolution fusion | flops 1077149696 | bytes 7340032 | tf_op jit(solution)/shard_map/dot_general | solution.py:123
  207.1 1.3 fusion.2
  208.4 1.3 fusion.3
  209.8 3.8 %fusion = bf16[2048,1536]{0,1:T(8,128)(2,1)} fusion(f32[2048,512]{0,1:T(8,128)S(1)} %fusion.24, f32[2048,512]{0,1:T(8,128)S(1)} %fusion.2, f32[2048,512]{0,1:T(8,128)S(1)} %fusion.3), kind=kLoop, calls=%fused_computation.1 | loop fusion | flops 12582912 | bytes 18874368 | tf_op jit(solution)/shard_map/convert_element_type | solution.py:158
  213.6 8.6 %copy.48 = bf16[2048,1536]{1,0:T(8,128)(2,1)} copy(bf16[2048,1536]{0,1:T(8,128)(2,1)} %fusion) | data formatting | bytes 12582912
  222.3 2.9 fusion.7
  225.1 4.2 %add_convert_fusion = bf16[512,2048]{1,0:T(8,128)(2,1)} fusion(f32[512,2048]{1,0:T(8,128)S(1)} %fusion.7, bf16[512,512]{1,0:T(8,128)(2,1)S(1)} %get-tuple-element.25, bf16[2048,1536]{1,0:T(8,128)(2,1)} %all-gather.3.cloned.1.call-done), kind=kOutput, calls=%fused_computation.2 | convolution fusion | flops 1075838976 | bytes 8912896 | tf_op jit(solution)/shard_map/dot_general | solution.py:51
  229.4 3.8 %all-to-all-start.1 = ((bf16[8,64,2048]{2,1,0:T(8,128)(2,1)}), bf16[8,64,2048]{2,1,0:T(8,128)(2,1)S(1)}, u32[]{:S(2)}, u32[]{:S(2)}) async-start(bf16[8,64,2048]{2,1,0:T(8,128)(2,1)} %bitcast.14), calls=%async_computation.2 | async-start | bytes 4194304 | tf_op jit(solution)/shard_map/all_to_all | solution.py:46
  236.8 23.5 %all-to-all-done.1 = bf16[8,64,2048]{2,1,0:T(8,128)(2,1)S(1)} async-done(((bf16[8,64,2048]{2,1,0:T(8,128)(2,1)}), bf16[8,64,2048]{2,1,0:T(8,128)(2,1)S(1)}, u32[]{:S(2)}, u32[]{:S(2)}) %all-to-all-start.1) | async-done | bytes 2097184 | tf_op jit(solution)/shard_map/all_to_all | solution.py:46
  262.6 2.2 fusion.23
  264.8 39.1 %reduce-scatter.7.cloned.1.call-done = bf16[128,1536]{1,0:T(8,128)(2,1)} async-done(((bf16[2048,1536]{1,0:T(8,128)(2,1)}), bf16[128,1536]{1,0:T(8,128)(2,1)}) %reduce-scatter.7.cloned.1.call-update) | async-done | bytes 393232
  (64 shorter events, 14.8 us)
Async XLA Ops:
  7.2 38.0 %all-gather.5.cloned.1.call-start = ((), (), s32[]{:S(2)}) async-start(), calls=%async_computation.5 | async-start | bytes 4718592 | tf_op jit(solution)/shard_map/all_gather | solution.py:86
  10.5 98.2 %all-gather.3.cloned.1.call-start = ((), (), s32[]{:S(2)}) async-start(), calls=%async_computation.4 | async-start | bytes 6684672 | tf_op jit(solution)/shard_map/all_gather | solution.py:17
  12.4 154.5 %reduce-scatter.5.cloned.1.call-start = ((), (), s32[]{:S(2)}) async-start(), calls=%async_computation.6 | async-start | bytes 4718592 | tf_op jit(solution)/shard_map/reduce_scatter | solution.py:99
  108.7 5.3 %copy-start = (bf16[2,512,2048]{2,1,0:T(8,128)(2,1)S(1)}, bf16[2,512,2048]{2,1,0:T(8,128)(2,1)}, u32[]{:S(2)}) copy-start(bf16[2,512,2048]{2,1,0:T(8,128)(2,1)} %all-gather.5.cloned.1.call-done) | copy-start | bytes 12582916
  108.7 5.9 %copy-start.2 = (bf16[2048,1536]{1,0:T(8,128)(2,1)S(1)}, bf16[2048,1536]{1,0:T(8,128)(2,1)}, u32[]{:S(2)}) copy-start(bf16[2048,1536]{1,0:T(8,128)(2,1)} %all-gather.3.cloned.1.call-done) | copy-start | bytes 18874372
  114.6 3.9 %copy-start.12 = (f32[1024,512]{1,0:T(8,128)}, f32[1024,512]{1,0:T(8,128)S(1)}, u32[]{:S(2)}) copy-start(f32[1024,512]{1,0:T(8,128)S(1)} %fusion.9) | copy-start | bytes 6291460
  129.2 0.7 copy-start.11
  129.2 41.9 %copy-start.3 = (bf16[64,2048]{1,0:T(8,128)(2,1)S(1)}, bf16[64,2048]{1,0:T(8,128)(2,1)}, u32[]{:S(2)}) copy-start(bf16[64,2048]{1,0:T(8,128)(2,1)} %param.13) | copy-start | bytes 786436
  129.3 174.6 %reduce-scatter.7.cloned.1.call-start = ((), (), s32[]{:S(2)}) async-start(), calls=%async_computation.7 | async-start | bytes 6684672
  201.6 1.6 copy-start.13
  201.6 2.2 copy-start.14
  203.8 3.3 %copy-start.1 = (bf16[2,512,2048]{2,1,0:T(8,128)(2,1)S(1)}, bf16[2,512,2048]{2,1,0:T(8,128)(2,1)}, u32[]{:S(2)}) copy-start(bf16[2,512,2048]{2,1,0:T(8,128)(2,1)} %all-gather.5.cloned.1.call-done) | copy-start | bytes 12582916
  229.4 3.8 %copy-start.7 = (f32[128,512]{1,0:T(8,128)S(1)}, f32[128,512]{1,0:T(8,128)}, u32[]{:S(2)}) copy-start(f32[128,512]{1,0:T(8,128)} %param.21) | copy-start | bytes 786436
  229.4 4.6 %copy-start.8 = (f32[128,512]{1,0:T(8,128)S(1)}, f32[128,512]{1,0:T(8,128)}, u32[]{:S(2)}) copy-start(f32[128,512]{1,0:T(8,128)} %param.20) | copy-start | bytes 786436
  229.4 5.5 %copy-start.9 = (f32[128,512]{1,0:T(8,128)S(1)}, f32[128,512]{1,0:T(8,128)}, u32[]{:S(2)}) copy-start(f32[128,512]{1,0:T(8,128)} %param.19) | copy-start | bytes 786436
  229.4 32.0 %copy-start.10 = (f32[2048]{0:T(1024)S(1)}, f32[2048]{0:T(1024)}, u32[]{:S(2)}) copy-start(f32[2048]{0:T(1024)} %param.14) | copy-start | bytes 24580
  229.4 30.9 %all-to-all-start.1 = ((bf16[8,64,2048]{2,1,0:T(8,128)(2,1)}), bf16[8,64,2048]{2,1,0:T(8,128)(2,1)S(1)}, u32[]{:S(2)}, u32[]{:S(2)}) async-start(bf16[8,64,2048]{2,1,0:T(8,128)(2,1)} %bitcast.14), calls=%async_computation.2 | async-start | bytes 4194304 | tf_op jit(solution)/shard_map/all_to_all | solution.py:46
  261.3 43.8 %copy-start.4 = (f32[128,512]{0,1:T(8,128)S(1)}, f32[128,512]{0,1:T(8,128)}, u32[]{:S(2)}) copy-start(f32[128,512]{0,1:T(8,128)} %copy.44) | copy-start | bytes 786436
  261.3 43.8 %copy-start.5 = (f32[128,512]{0,1:T(8,128)S(1)}, f32[128,512]{0,1:T(8,128)}, u32[]{:S(2)}) copy-start(f32[128,512]{0,1:T(8,128)} %copy.43) | copy-start | bytes 786436
  261.3 43.8 %copy-start.6 = (f32[128,512]{0,1:T(8,128)S(1)}, f32[128,512]{0,1:T(8,128)}, u32[]{:S(2)}) copy-start(f32[128,512]{0,1:T(8,128)} %copy.42) | copy-start | bytes 786436
Sparse Core Ops, SparseCore 0:
  10.6 34.4 all-gather.4
  47.3 61.3 all-gather.2
  129.4 37.4 reduce-scatter.4
  222.4 81.4 reduce-scatter.6
where the time goes:
time: 315 us; the launch traced here: 314 us
  waiting for transfers between devices  196 us (62%)
  blocking collectives  29.7 us (9%)
  matrix products  27.9 us (9%)
  local copies, waits for them, and re-layouts  27.4 us (9%)
  other arithmetic  15.7 us (5%)
  between operations  13.9 us (4%)
  starting transfers between devices  3.91 us (1%)
    all_gather x1, waiting for transfers between devices, sent_together(): lax.all_gather(both, axis, axis=dim, tiled=True)  63.5 us
    unnamed x5, waiting for transfers between devices  39.1 us
    reduce_scatter x1, waiting for transfers between devices, per_device(): lax.psum_scatter(gated_product.reshape(lax.axis_size('tp') * tok_rows, 2...  36.9 us
    all_gather x1, waiting for transfers between devices, per_device(): normed_rows = lax.all_gather(normed, 'tp', axis=1, tiled=True)  32.7 us
    all_to_all x1, blocking collectives, sent_to_all(): lax.all_to_all(jnp.broadcast_to(shard[None], (peers, *shard.shape)), axis...  29.7 us
    all_to_all x1, waiting for transfers between devices, summed_on_arrival(): lax.all_to_all(parts, axis, split_axis=0, concat_axis=0, tiled=True)  23.5 us
    unnamed x39, local copies, waits for them, and re-layouts  17.1 us
    dot_general x2, matrix products, contract_last(): lax.dot_general(first_op, second_op, (((1,), (1,)), ((), ())), preferred_...  7.09 us
  transfers between devices with their start and end apart: 5, of which 5 were waited for; matrix products, arithmetic and copies ran while one was open for 5% of the time, Pallas kernels for 0%

commit v1 on v0

v1 whole, which is shorter than its diff:
```python
import math

import jax
import jax.numpy as jnp
from jax import lax
from jax.experimental import pallas as pl
from jax.experimental.pallas import tpu as pltpu
from jax.sharding import PartitionSpec as P

NORM_EPS = 1e-06
BF = jnp.bfloat16
F32 = jnp.float32
MESH = pl.DeviceIdType.MESH

ORDER = [
    (0, 0), (0, 1), (0, -1), (1, 0),
    (-1, 0), (2, 0), (1, 1), (1, -1),
    (-1, 1), (-1, -1), (0, 2), (1, 2),
    (-1, 2), (2, 1), (2, -1), (2, 2),
]
HOPS = (
    [((0, 0), ax, sg, None) for ax in "ab" for sg in (1, -1)]
    + [((2, 0), "b", sg, None) for sg in (1, -1)]
    + [((0, s), "a", sg, None) for s in (1, -1) for sg in (1, -1)]
    + [((0, s), "b", -s, (1 + s) // 2) for s in (1, -1)]
    + [((s, t), "b", -t, (1 + t) // 2) for s in (1, -1) for t in (1, -1)]
    + [((s, 0), "a", -s, (1 + s) // 2) for s in (1, -1)]
    + [((s, 2), "a", -s, (1 + s) // 2) for s in (1, -1)]
)


def wrapped(n):
    n %= 4
    return n - 4 if n == 3 else n


def landing(hop):
    (da, db), ax, sg, _ = hop
    if ax == "a":
        da -= sg
    else:
        db -= sg
    return (wrapped(db), wrapped(da))


LANDS = [ORDER.index(landing(hop)) for hop in HOPS]
ARRIVALS = {o: [i for i, k in enumerate(LANDS) if ORDER[k] == o] for o in ORDER}
DUTIES = {o: [i for i, hop in enumerate(HOPS) if hop[0] == o] for o in ORDER}
SLOT, _at = [], 0
for _hop in HOPS:
    SLOT.append(_at)
    _at += 128 if _hop[3] is None else 64
ARRIVED_ROWS = _at


def rows_of(k, part):
    return (k * 128, 128) if part is None else (k * 128 + 64 * part, 64)


def last_last(a, b):
    return lax.dot_general(a, b, (((1,), (1,)), ((), ())), preferred_element_type=F32)


def first_first(a, b):
    return lax.dot_general(a, b, (((0,), (0,)), ((), ())), preferred_element_type=F32)


def kernel(
    late_in, early_in, early_grad, pre_gain, post_gain, gate_w, up_w, down_w,
    gate_sum, up_sum, down_sum,
    late_out, early_out, gate_out, up_out, down_out,
    w_all, tok, tok_t, pre, dgate, dup, hid, part, pair, both, fwd, last, cot, hcot,
    gcot, ucot, grads, arrived, mixed, weighted,
    ag_s, ag_r, rs_s, rs_r, xa_s, xa_r, xr_s, xr_r,
):
    fs = lax.axis_index("fs")
    tp = lax.axis_index("tp")
    y, z = fs % 4, fs // 4
    par = (y + z) % 2
    core, x = tp % 2, tp // 2
    grad_scale = 1.0 / math.sqrt(8192.0)

    def fs_at(da, db):
        dy = (1 - par) * da + par * db
        dz = (1 - par) * db + par * da
        return ((z + dz + 4) % 4) * 4 + (y + dy + 4) % 4

    def torus(ax, sg):
        return (fs_at(sg, 0) if ax == "a" else fs_at(0, sg), tp)

    ring = {sg: (fs, ((x + sg + 4) % 4) * 2 + core) for sg in (1, -1)}
    partner = (fs, x * 2 + 1 - core)
    columns = [pl.multiple_of(fs_at(*o) * 128, 128) for o in ORDER]

    barrier = pltpu.get_barrier_semaphore()
    peers = [partner, ring[1], ring[-1]] + [torus(ax, sg) for ax in "ab" for sg in (1, -1)]
    for peer in peers:
        pl.semaphore_signal(barrier, inc=1, device_id=peer, device_id_type=MESH)
    pl.semaphore_wait(barrier, len(peers))

    sent = []

    def send(src, dst, ss, rs, to):
        copy = pltpu.make_async_remote_copy(
            src_ref=src, dst_ref=dst, send_sem=ss, recv_sem=rs,
            device_id=to, device_id_type=MESH,
        )
        copy.start()
        sent.append(copy)

    def arrive(dst, ss, rs):
        pltpu.make_async_remote_copy(
            src_ref=dst, dst_ref=dst, send_sem=ss, recv_sem=rs,
            device_id=partner, device_id_type=MESH,
        ).wait_recv()

    own_w = (gate_w, up_w, down_w)

    def pass_on(w, offset):
        for i in DUTIES[offset]:
            _, ax, sg, q = HOPS[i]
            start, n = rows_of(ORDER.index(offset), q)
            src = own_w[w] if offset == (0, 0) else w_all.at[w, pl.ds(start, n)]
            there, _ = rows_of(LANDS[i], q)
            send(src, w_all.at[w, pl.ds(there, n)], ag_s.at[w, i], ag_r.at[w, i], torus(ax, sg))

    def take(w, offset):
        for i in ARRIVALS[offset]:
            start, n = rows_of(LANDS[i], HOPS[i][3])
            arrive(w_all.at[w, pl.ds(start, n)], ag_s.at[w, i], ag_r.at[w, i])

    def relay(w, offsets):
        for offset in offsets:
            take(w, offset)
            pass_on(w, offset)

    near = [(0, 1), (0, -1), (1, 0), (-1, 0)]
    mid = [(2, 0), (1, 1), (1, -1), (-1, 1), (-1, -1), (0, 2)]
    far = [(1, 2), (-1, 2), (2, 1), (2, -1)]
    end = [(2, 2)]

    def spread(j, view):
        send(view(0, 64), view(192, 64), xa_s.at[j, 0], xa_r.at[j, 0], ring[1])
        send(view(0, 64), view(64, 64), xa_s.at[j, 1], xa_r.at[j, 1], ring[-1])
        send(view(0, 64), view(256, 64), xa_s.at[j, 4], xa_r.at[j, 4], partner)

    def spread_near(j, view):
        arrive(view(192, 64), xa_s.at[j, 0], xa_r.at[j, 0])
        send(view(192, 32), view(128, 32), xa_s.at[j, 2], xa_r.at[j, 2], ring[1])
        send(view(192, 64), view(448, 64), xa_s.at[j, 7], xa_r.at[j, 7], partner)
        arrive(view(64, 64), xa_s.at[j, 1], xa_r.at[j, 1])
        send(view(96, 32), view(160, 32), xa_s.at[j, 3], xa_r.at[j, 3], ring[-1])
        send(view(64, 64), view(320, 64), xa_s.at[j, 5], xa_r.at[j, 5], partner)

    def spread_far(j, view):
        arrive(view(128, 32), xa_s.at[j, 2], xa_r.at[j, 2])
        arrive(view(160, 32), xa_s.at[j, 3], xa_r.at[j, 3])
        send(view(128, 64), view(384, 64), xa_s.at[j, 6], xa_r.at[j, 6], partner)

    def spread_end(j, view):
        for i, row in ((4, 256), (5, 320), (7, 448), (6, 384)):
            arrive(view(row, 64), xa_s.at[j, i], xa_r.at[j, i])

    def tok_view(m):
        return lambda row, n: tok.at[m, pl.ds(row, n)]

    def cot_view(g):
        return lambda row, n: cot.at[pl.ds(row, n), pl.ds(512 * g, 512)]

    def sum_pair(v, g):
        s = 4 * v + g
        send(part.at[v, g, pl.ds(256, 256)], pair.at[v, g], xr_s.at[s, 0], xr_r.at[s, 0], partner)

    def sum_start(v, g):
        s = 4 * v + g
        arrive(pair.at[v, g], xr_s.at[s, 0], xr_r.at[s, 0])
        both[v, g] = (part[v, g, :256].astype(F32) + pair[v, g].astype(F32)).astype(BF)
        send(
            both.at[v, g, pl.ds(128, 32)], fwd.at[v, g, pl.ds(0, 32)],
            xr_s.at[s, 1], xr_r.at[s, 1], ring[1],
        )
        send(
            both.at[v, g, pl.ds(160, 32)], fwd.at[v, g, pl.ds(32, 32)],
            xr_s.at[s, 2], xr_r.at[s, 2], ring[-1],
        )

    def sum_middle(v, g):
        s = 4 * v + g
        arrive(fwd.at[v, g, pl.ds(0, 32)], xr_s.at[s, 1], xr_r.at[s, 1])
        both[v, g, 64:96] = (both[v, g, 64:96].astype(F32) + fwd[v, g, :32].astype(F32)).astype(BF)
        send(
            both.at[v, g, pl.ds(64, 64)], last.at[v, g, pl.ds(0, 64)],
            xr_s.at[s, 3], xr_r.at[s, 3], ring[1],
        )
        arrive(fwd.at[v, g, pl.ds(32, 32)], xr_s.at[s, 2], xr_r.at[s, 2])
        both[v, g, 224:256] = (
            both[v, g, 224:256].astype(F32) + fwd[v, g, 32:].astype(F32)
        ).astype(BF)
        send(
            both.at[v, g, pl.ds(192, 64)], last.at[v, g, pl.ds(64, 64)],
            xr_s.at[s, 4], xr_r.at[s, 4], ring[-1],
        )

    def sum_end(v, g):
        s = 4 * v + g
        arrive(last.at[v, g, pl.ds(0, 64)], xr_s.at[s, 3], xr_r.at[s, 3])
        arrive(last.at[v, g, pl.ds(64, 64)], xr_s.at[s, 4], xr_r.at[s, 4])
        total = both[v, g, :64].astype(F32) + last[v, g, :64].astype(F32)
        mixed[v, :, pl.ds(512 * g, 512)] = (total + last[v, g, 64:].astype(F32)).astype(BF)

    def give(w, offset):
        k = ORDER.index(offset)
        for i in ARRIVALS[offset]:
            _, ax, sg, q = HOPS[i]
            start, n = rows_of(k, q)
            send(
                grads.at[w, pl.ds(start, n)], arrived.at[w, pl.ds(SLOT[i], n)],
                rs_s.at[w, i], rs_r.at[w, i], torus("b" if ax == "a" else "a", -sg),
            )

    def gain(w, offset):
        k = ORDER.index(offset)
        for i in DUTIES[offset]:
            start, n = rows_of(k, HOPS[i][3])
            arrive(arrived.at[w, pl.ds(SLOT[i], n)], rs_s.at[w, i], rs_r.at[w, i])
        halves = [i for i in DUTIES[offset] if HOPS[i][3] is not None]
        wholes = [i for i in DUTIES[offset] if HOPS[i][3] is None]
        for q in (0, 1):
            terms = [SLOT[i] + 64 * q for i in wholes]
            terms += [SLOT[i] for i in halves if HOPS[i][3] == q]
            if terms:
                start, _ = rows_of(k, q)
                total = grads[w, start : start + 64].astype(F32)
                for at in terms:
                    total += arrived[w, at : at + 64].astype(F32)
                grads[w, start : start + 64] = total.astype(BF)

    def combine(w, offsets):
        for offset in offsets:
            gain(w, offset)
            give(w, offset)

    def finish(w, old, out):
        for i in DUTIES[(0, 0)]:
            arrive(arrived.at[w, pl.ds(SLOT[i], 128)], rs_s.at[w, i], rs_r.at[w, i])
        for q in (0, 1):
            total = grads[w, 64 * q : 64 * q + 64].astype(F32)
            for i in DUTIES[(0, 0)]:
                at = SLOT[i] + 64 * q
                total += arrived[w, at : at + 64].astype(F32)
            out[64 * q : 64 * q + 64] = old[64 * q : 64 * q + 64] + grad_scale * total

    def tiles(count, body):
        lax.fori_loop(0, count, lambda i, c: (body(i), c)[1], 0)

    def norm_tokens(m, source):
        values = source[...].astype(F32)
        inverse = lax.rsqrt(jnp.mean(values * values, axis=-1, keepdims=True) + NORM_EPS)
        for k, at in enumerate(columns):
            tok[m, 0:64, 128 * k : 128 * k + 128] = (
                source[:, pl.ds(at, 128)].astype(F32) * inverse * pre_gain[:, pl.ds(at, 128)]
            ).astype(BF)

    def gate_product(m):
        def body(i):
            r = pl.multiple_of(i * 128, 128)
            pre[m, pl.ds(r, 128)] = jnp.dot(
                tok[m, pl.ds(r, 128)], w_all[0], preferred_element_type=F32
            )

        tiles(4, body)

    def up_product(m):
        def body(i):
            r = pl.multiple_of(i * 128, 128)
            up = jnp.dot(tok[m, pl.ds(r, 128)], w_all[1], preferred_element_type=F32)
            gate = pre[m, pl.ds(r, 128)]
            s = jax.nn.sigmoid(gate)
            hid[m, pl.ds(r, 128)] = (gate * s * up).astype(BF)
            if m == 1:
                dgate[pl.ds(r, 128)] = up * s * (1.0 + gate * (1.0 - s))
                dup[pl.ds(r, 128)] = gate * s

        tiles(4, body)

    def down_product(m, v, g):
        def body(i):
            r = pl.multiple_of(i * 256, 256)
            part[v, g, pl.ds(r, 256)] = last_last(
                hid[m, pl.ds(r, 256)], w_all[2, pl.ds(512 * g, 512)]
            ).astype(BF)

        tiles(2, body)

    def back_product(g):
        def body(i):
            r = pl.multiple_of(i * 256, 256)
            part[2, g, pl.ds(r, 256)] = (
                last_last(gcot[pl.ds(r, 256)], w_all[0, pl.ds(512 * g, 512)])
                + last_last(ucot[pl.ds(r, 256)], w_all[1, pl.ds(512 * g, 512)])
            ).astype(BF)

        tiles(2, body)

    def hidden_product(g, first):
        def body(i):
            r = pl.multiple_of(i * 256, 256)
            term = jnp.dot(
                cot[pl.ds(r, 256), pl.ds(512 * g, 512)],
                w_all[2, pl.ds(512 * g, 512)],
                preferred_element_type=F32,
            )
            hcot[pl.ds(r, 256)] = term if first else hcot[pl.ds(r, 256)] + term

        tiles(2, body)

    def down_gradient(g):
        grads[2, pl.ds(512 * g, 512)] = first_first(
            cot[:, pl.ds(512 * g, 512)], hid[1]
        ).astype(BF)

    def turn_tokens():
        for k in range(16):
            tok_t[128 * k : 128 * k + 128] = tok[1, :, 128 * k : 128 * k + 128].T

    def weight_gradient(w, g, values):
        def body(i):
            r = pl.multiple_of(512 * g + i * 256, 256)
            grads[w, pl.ds(r, 256)] = jnp.dot(
                tok_t[pl.ds(r, 256)], values[...], preferred_element_type=F32
            ).astype(BF)

        tiles(2, body)

    pass_on(0, (0, 0))
    norm_tokens(1, early_in)
    spread(1, tok_view(1))
    pass_on(1, (0, 0))
    norm_tokens(0, late_in)
    spread(0, tok_view(0))
    for w in range(3):
        w_all[w, 0:128] = own_w[w][...]
    for k, at in enumerate(columns):
        weighted[:, 128 * k : 128 * k + 128] = (
            0.5 * early_grad[:, pl.ds(at, 128)].astype(F32) * post_gain[:, pl.ds(at, 128)]
        )
    relay(0, near)
    spread_near(1, tok_view(1))
    relay(1, near)
    pass_on(2, (0, 0))
    relay(0, mid)
    spread_far(1, tok_view(1))
    relay(0, far)
    relay(2, near)
    relay(1, mid)
    spread_near(0, tok_view(0))
    relay(0, end)
    spread_end(1, tok_view(1))
    gate_product(1)
    relay(1, far)
    spread_far(0, tok_view(0))
    relay(2, mid)
    turn_tokens()
    relay(1, end)
    up_product(1)
    down_product(1, 0, 0)
    sum_pair(0, 0)
    down_product(1, 0, 1)
    sum_pair(0, 1)
    relay(2, far)
    sum_start(0, 0)
    down_product(1, 0, 2)
    sum_pair(0, 2)
    sum_start(0, 1)
    spread_end(0, tok_view(0))
    gate_product(0)
    sum_middle(0, 0)
    sum_start(0, 2)
    sum_middle(0, 1)
    relay(2, end)
    down_product(1, 0, 3)
    sum_pair(0, 3)
    sum_middle(0, 2)
    sum_end(0, 0)
    sum_start(0, 3)
    sum_end(0, 1)
    up_product(0)
    sum_middle(0, 3)
    sum_end(0, 2)
    down_product(0, 1, 0)
    sum_pair(1, 0)
    sum_end(0, 3)

    values = mixed[0].astype(F32)
    inverse = lax.rsqrt(jnp.mean(values * values, axis=-1, keepdims=True) + NORM_EPS)
    scaled = inverse**3 * jnp.mean(weighted[...] * values, axis=-1, keepdims=True)
    cot[0:64] = (inverse * weighted[...] - values * scaled).astype(BF)
    for g in (3, 2, 1, 0):
        spread(g + 2, cot_view(g))
    for g in (1, 2, 3):
        down_product(0, 1, g)
        sum_pair(1, g)
    for g in (3, 2, 1, 0):
        spread_near(g + 2, cot_view(g))
        spread_far(g + 2, cot_view(g))
        spread_end(g + 2, cot_view(g))
        down_gradient(g)
        if g == 3:
            for o in end + [(2, 1), (2, -1)]:
                give(2, o)
        if g == 2:
            give(2, (0, 2))
        hidden_product(g, g == 3)
        sum_start(1, g)
    combine(2, [(1, 2), (-1, 2)])

    gcot[...] = (hcot[...] * dgate[...]).astype(BF)
    ucot[...] = (hcot[...] * dup[...]).astype(BF)
    for w, values_of in ((0, gcot), (1, ucot)):
        weight_gradient(w, 3, values_of)
        for o in end + [(2, 1), (2, -1)]:
            give(w, o)
        weight_gradient(w, 2, values_of)
        give(w, (0, 2))
        if w == 0:
            combine(2, [(1, 1), (1, -1), (-1, 1), (-1, -1)])
        weight_gradient(w, 1, values_of)
        weight_gradient(w, 0, values_of)
        if w == 0:
            combine(2, [(2, 0), (1, 0), (-1, 0)])
            combine(0, [(1, 2), (-1, 2)])
    for g in range(4):
        back_product(g)
        sum_pair(2, g)
    for g in (3, 2, 1, 0):
        sum_middle(1, g)
    combine(0, [(1, 1), (1, -1), (-1, 1), (-1, -1)])
    combine(1, [(1, 2), (-1, 2)])
    combine(2, [(0, 1), (0, -1)])
    combine(0, [(2, 0), (1, 0), (-1, 0)])
    for g in range(4):
        sum_end(1, g)
        sum_start(2, g)
    combine(1, [(1, 1), (1, -1), (-1, 1), (-1, -1)])

    late_mixed = mixed[1].astype(F32)
    late_inverse = lax.rsqrt(jnp.mean(late_mixed * late_mixed, axis=-1, keepdims=True) + NORM_EPS)
    for k, at in enumerate(columns):
        late_out[:, pl.ds(at, 128)] = (
            late_in[:, pl.ds(at, 128)].astype(F32)
            + 0.5
            * mixed[1, :, 128 * k : 128 * k + 128].astype(F32)
            * late_inverse
            * post_gain[:, pl.ds(at, 128)]
        ).astype(BF)

    combine(0, [(0, 1), (0, -1)])
    combine(1, [(2, 0), (1, 0), (-1, 0)])
    for g in range(4):
        sum_middle(2, g)
    finish(2, down_sum, down_out)
    combine(1, [(0, 1), (0, -1)])
    for g in range(4):
        sum_end(2, g)

    early = early_in[...].astype(F32)
    early_inverse = lax.rsqrt(jnp.mean(early * early, axis=-1, keepdims=True) + NORM_EPS)
    dots = jnp.zeros((64, 128), F32)
    for k, at in enumerate(columns):
        dots += (
            mixed[2, :, 128 * k : 128 * k + 128].astype(F32)
            * pre_gain[:, pl.ds(at, 128)]
            * early_in[:, pl.ds(at, 128)].astype(F32)
        )
    slope = early_inverse**3 * (jnp.sum(dots, axis=-1, keepdims=True) * (1.0 / 2048.0))
    for k, at in enumerate(columns):
        early_out[:, pl.ds(at, 128)] = (
            early_grad[:, pl.ds(at, 128)].astype(F32)
            + early_inverse
            * (mixed[2, :, 128 * k : 128 * k + 128].astype(F32) * pre_gain[:, pl.ds(at, 128)])
            - early_in[:, pl.ds(at, 128)].astype(F32) * slope
        ).astype(BF)

    finish(0, gate_sum, gate_out)
    finish(1, up_sum, up_out)
    for copy in sent:
        copy.wait_send()


def per_device(
    late_input,
    early_input,
    early_grad,
    pre_gain,
    post_gain,
    gate_weight,
    up_weight,
    down_weight,
    gate_sum,
    up_sum,
    down_gradient_sum,
):
    sem = pltpu.SemaphoreType.DMA
    vmem = pltpu.VMEM
    tokens = jax.ShapeDtypeStruct((64, 2048), BF)
    total = jax.ShapeDtypeStruct((128, 512), F32)
    return pl.pallas_call(
        kernel,
        name="half_step",
        out_shape=(tokens, tokens, total, total, total),
        in_specs=[pl.BlockSpec(memory_space=vmem)] * 11,
        out_specs=[pl.BlockSpec(memory_space=vmem)] * 5,
        scratch_shapes=[
            vmem((3, 2048, 512), BF),
            vmem((2, 512, 2048), BF),
            vmem((2048, 512), BF),
            vmem((2, 512, 512), F32),
            vmem((512, 512), F32),
            vmem((512, 512), F32),
            vmem((2, 512, 512), BF),
            vmem((3, 4, 512, 512), BF),
            vmem((3, 4, 256, 512), BF),
            vmem((3, 4, 256, 512), BF),
            vmem((3, 4, 64, 512), BF),
            vmem((3, 4, 128, 512), BF),
            vmem((512, 2048), BF),
            vmem((512, 512), F32),
            vmem((512, 512), BF),
            vmem((512, 512), BF),
            vmem((3, 2048, 512), BF),
            vmem((3, ARRIVED_ROWS, 512), BF),
            vmem((3, 64, 2048), BF),
            vmem((64, 2048), F32),
            sem((3, 20)),
            sem((3, 20)),
            sem((3, 20)),
            sem((3, 20)),
            sem((6, 8)),
            sem((6, 8)),
            sem((12, 5)),
            sem((12, 5)),
        ],
        compiler_params=pltpu.CompilerParams(
            collective_id=0, has_side_effects=True, vmem_limit_bytes=67043328
        ),
    )(
        late_input, early_input, early_grad, pre_gain.reshape(1, -1), post_gain.reshape(1, -1),
        gate_weight, up_weight, down_weight, gate_sum, up_sum, down_gradient_sum,
    )


def solution(mesh):
    rows, both = P(("fs", "tp"), None), P("fs", "tp")
    return jax.shard_map(
        per_device,
        mesh=mesh,
        in_specs=(rows,) * 3 + (P(), P()) + (both,) * 6,
        out_specs=(rows, rows, both, both, both),
        check_vma=False,
    )
```

time: 315 us -> 139 us (0.44)
  waiting for transfers between devices: 196 us -> 0 us
  Pallas kernels: 0 us -> 133 us
  blocking collectives: 29.7 us -> 0 us
  matrix products: 27.9 us -> 0 us
  local copies, waits for them, and re-layouts: 27.4 us -> 5.55 us
  other arithmetic: 15.7 us -> 0 us
  between operations: 13.9 us -> 0.66 us
  starting transfers between devices: 3.91 us -> 0 us
    pallas_call x0 -> x1, Pallas kernels: none -> 133 us  [per_device(): pl.pallas_call(kernel, name='half_step', out_shape=(tokens, tokens, total...]
    all_gather x2 -> x0, waiting for transfers between devices: 96.3 us -> none  [the longest x1 63.5 us: sent_together(): lax.all_gather(both, axis, axis=dim, tiled=True)]
    unnamed x5 -> x0, waiting for transfers between devices: 39.1 us -> none
    reduce_scatter x1 -> x0, waiting for transfers between devices: 36.9 us -> none  [per_device(): lax.psum_scatter(gated_product.reshape(lax.axis_size('tp') * tok_rows, 2...]
    all_to_all x1 -> x0, blocking collectives: 29.7 us -> none  [sent_to_all(): lax.all_to_all(jnp.broadcast_to(shard[None], (peers, *shard.shape)), axis...]
    dot_general x9 -> x0, matrix products: 27.9 us -> none  [the longest x2 7.09 us: contract_last(): lax.dot_general(first_op, second_op, (((1,), (1,)), ((), ())), preferred_...]
    all_to_all x1 -> x0, waiting for transfers between devices: 23.5 us -> none  [summed_on_arrival(): lax.all_to_all(parts, axis, split_axis=0, concat_axis=0, tiled=True)]
    unnamed x39 -> x13, local copies, waits for them, and re-layouts: 17.1 us -> 5.55 us
  transfers between devices with their start and end apart: 5 -> 0, of which waited for: 5 -> 0; matrix products, arithmetic and copies ran while one was open for 5% -> 0% of each run, Pallas kernels for 0% -> 0%
where the time goes in v1:
time: 139 us
  Pallas kernels  133 us (96%)
  local copies, waits for them, and re-layouts  5.55 us (4%)
    pallas_call x1, Pallas kernels, per_device(): pl.pallas_call(kernel, name='half_step', out_shape=(tokens, tokens, total...  133 us
    unnamed x13, local copies, waits for them, and re-layouts  5.55 us

profile of v1, /device:TPU:0, one launch (start us, length us, event | category | flops | bytes accessed | tf_op | source)
XLA Modules:
  0.0 139.2 jit_solution(2632412629656969377)
XLA Ops:
  0.6 133.0 %half_step.1 = (bf16[64,2048]{1,0:T(8,128)(2,1)}, bf16[64,2048]{1,0:T(8,128)(2,1)}, f32[128,512]{1,0:T(8,128)}, f32[128,512]{1,0:T(8,128)}, f32[128,512]{1,0:T(8,128)}) custom-call(bf16[64,2048]{1,0:T(8,128)(2,1)} %late_in.1, bf16[64,2048]{1,0:T(8,128)(2,1)} %early_in.1, bf16[64,2048]{1,0:T(8,128)(2,1)} %early_grad.1, f32[1,2048]{1,0:T(1,128)} %bitcast.2, ...), custom_call_target="tpu_custom_call" | custom-call | tf_op jit(solution)/shard_map/half_step/pallas_call | solution.py:507
  133.6 0.0 copy-start.3
  133.6 1.7 %copy.21 = bf16[64,2048]{1,0:T(8,128)(2,1)} copy(bf16[64,2048]{1,0:T(8,128)(2,1)} %get-tuple-element.10) | data formatting | bytes 524288
  135.3 0.0 copy-done.3
  135.3 0.0 copy-start.2
  135.3 0.7 copy.22
  136.0 0.3 copy-done.2
  136.4 0.0 copy-start.1
  136.4 0.7 copy.23
  137.1 0.3 copy-done.1
  137.4 0.0 copy-start
  137.4 0.7 copy.24
  138.1 0.3 copy-done
  138.5 0.7 copy.25
Async XLA Ops:
  133.6 1.7 %copy-start.3 = (bf16[64,2048]{1,0:T(8,128)(2,1)S(1)}, bf16[64,2048]{1,0:T(8,128)(2,1)}, u32[]{:S(2)}) copy-start(bf16[64,2048]{1,0:T(8,128)(2,1)} %get-tuple-element.11) | copy-start | bytes 786436
  135.3 1.0 copy-start.2
  136.4 1.0 copy-start.1
  137.4 1.0 copy-start

commit v2 on v0

v2 whole, which is shorter than its diff:
```python
import math

import jax
import jax.numpy as jnp
from jax import lax
from jax.experimental import pallas as pl
from jax.experimental.pallas import tpu as pltpu
from jax.sharding import PartitionSpec as P

NORM_EPS = 1e-06
BF = jnp.bfloat16
F32 = jnp.float32
MESH = pl.DeviceIdType.MESH

ORDER = [
    (0, 0), (0, 1), (0, -1), (1, 0),
    (-1, 0), (2, 0), (1, 1), (1, -1),
    (-1, 1), (-1, -1), (0, 2), (1, 2),
    (-1, 2), (2, 1), (2, -1), (2, 2),
]
HOPS = (
    [((0, 0), ax, sg, None) for ax in "ab" for sg in (1, -1)]
    + [((2, 0), "b", sg, None) for sg in (1, -1)]
    + [((0, s), "a", sg, None) for s in (1, -1) for sg in (1, -1)]
    + [((0, s), "b", -s, (1 + s) // 2) for s in (1, -1)]
    + [((s, t), "b", -t, (1 + t) // 2) for s in (1, -1) for t in (1, -1)]
    + [((s, 0), "a", -s, (1 + s) // 2) for s in (1, -1)]
    + [((s, 2), "a", -s, (1 + s) // 2) for s in (1, -1)]
)


(
    OWN, RELAY, NORM, SPREAD, NEAR, FAR, FULL, WEIGH, GATE, UP, DOWN, BACK, START, MIDDLE,
    SUMMED, TURN, COT, HIDDEN, DGRAD, DERIVE, WGRAD, COMBINE, LATE, EARLY,
) = range(24)
SCRIPT = [
    (NORM, 1), (SPREAD, 1), (OWN, 0), (NORM, 0), (OWN, 1), (SPREAD, 0), (OWN, 2), (OWN, 3),
    (WEIGH,), (RELAY, 0, 1), (RELAY, 0, 3), (RELAY, 0, 4), (RELAY, 0, 2), (RELAY, 1, 1),
    (RELAY, 1, 3), (RELAY, 1, 4), (RELAY, 1, 2), (RELAY, 2, 1), (RELAY, 2, 3), (RELAY, 2, 4),
    (RELAY, 2, 2), (NEAR, 1, -1), (NEAR, 1, 1), (RELAY, 3, 1), (RELAY, 3, 3), (RELAY, 3, 4),
    (RELAY, 3, 2), (RELAY, 0, 5), (RELAY, 0, 6), (RELAY, 0, 7), (RELAY, 1, 6), (RELAY, 0, 10),
    (RELAY, 1, 7), (RELAY, 1, 10), (RELAY, 0, 8), (RELAY, 0, 9), (RELAY, 1, 8), (RELAY, 1, 5),
    (RELAY, 1, 9), (RELAY, 2, 5), (NEAR, 0, -1), (NEAR, 0, 1), (RELAY, 2, 6), (RELAY, 2, 7),
    (RELAY, 3, 6), (RELAY, 2, 10), (RELAY, 3, 7), (RELAY, 3, 10), (RELAY, 2, 8), (RELAY, 2, 9),
    (OWN, 4), (FAR, 1), (RELAY, 3, 5), (RELAY, 3, 8), (RELAY, 3, 9), (OWN, 5), (RELAY, 1, 13),
    (RELAY, 0, 11), (RELAY, 0, 12), (FULL, 1), (TURN,), (RELAY, 0, 13), (RELAY, 1, 12), (FAR, 0),
    (RELAY, 0, 14), (RELAY, 1, 11), (RELAY, 1, 14), (RELAY, 3, 13), (RELAY, 2, 11),
    (RELAY, 2, 12), (FULL, 0), (RELAY, 2, 13), (RELAY, 4, 1), (RELAY, 4, 2), (RELAY, 2, 14),
    (RELAY, 3, 11), (RELAY, 3, 12), (RELAY, 3, 14), (RELAY, 4, 3), (RELAY, 4, 4), (RELAY, 5, 1),
    (RELAY, 5, 3), (RELAY, 5, 4), (RELAY, 5, 2), (RELAY, 0, 15), (RELAY, 1, 15), (GATE, 1, 0),
    (GATE, 1, 1), (RELAY, 2, 15), (RELAY, 4, 5), (GATE, 1, 2), (RELAY, 3, 15), (GATE, 1, 3),
    (UP, 1, 0), (RELAY, 4, 6), (RELAY, 4, 7), (UP, 1, 1), (UP, 1, 2), (RELAY, 5, 6),
    (RELAY, 5, 7), (UP, 1, 3), (RELAY, 4, 8), (RELAY, 4, 9), (DOWN, 0, 0), (RELAY, 4, 10),
    (RELAY, 5, 10), (GATE, 0, 0), (RELAY, 5, 5), (GATE, 0, 1), (RELAY, 5, 8), (DOWN, 0, 1),
    (RELAY, 5, 9), (GATE, 0, 2), (START, 0, 0), (RELAY, 4, 11), (RELAY, 4, 12), (RELAY, 5, 13),
    (DOWN, 0, 2), (RELAY, 4, 13), (GATE, 0, 3), (START, 0, 1), (UP, 0, 0), (RELAY, 4, 14),
    (UP, 0, 1), (RELAY, 5, 11), (RELAY, 5, 12), (UP, 0, 2), (START, 0, 2), (UP, 0, 3),
    (MIDDLE, 0, 0, -1), (MIDDLE, 0, 0, 1), (RELAY, 5, 14), (DOWN, 1, 0), (RELAY, 4, 15),
    (DOWN, 1, 1), (MIDDLE, 0, 1, -1), (MIDDLE, 0, 1, 1), (DOWN, 1, 2), (RELAY, 5, 15),
    (DOWN, 0, 3), (MIDDLE, 0, 2, -1), (MIDDLE, 0, 2, 1), (DOWN, 1, 3), (SUMMED, 0, 0),
    (START, 0, 3), (SUMMED, 0, 1), (SUMMED, 0, 2), (SUMMED, 0, 3), (COT,), (SPREAD, 5),
    (SPREAD, 4), (SPREAD, 3), (SPREAD, 2), (NEAR, 5, -1), (FAR, 5), (NEAR, 4, -1), (NEAR, 5, 1),
    (NEAR, 3, -1), (FULL, 5), (DGRAD, 3), (NEAR, 4, 1), (NEAR, 2, -1), (COMBINE, 4, 15),
    (COMBINE, 5, 15), (COMBINE, 4, 13), (COMBINE, 4, 14), (COMBINE, 5, 14), (HIDDEN, 3),
    (NEAR, 3, 1), (START, 1, 0), (START, 1, 1), (START, 1, 2), (START, 1, 3), (NEAR, 2, 1),
    (FAR, 4), (COMBINE, 4, 12), (COMBINE, 5, 11), (COMBINE, 5, 12), (FAR, 3), (MIDDLE, 1, 0, -1),
    (FULL, 4), (DGRAD, 2), (COMBINE, 5, 13), (COMBINE, 4, 10), (COMBINE, 4, 11), (COMBINE, 4, 8),
    (COMBINE, 4, 9), (COMBINE, 5, 9), (HIDDEN, 2), (FULL, 3), (DGRAD, 1), (COMBINE, 5, 10),
    (COMBINE, 4, 6), (COMBINE, 4, 7), (COMBINE, 5, 8), (HIDDEN, 1), (MIDDLE, 1, 0, 1),
    (MIDDLE, 1, 1, -1), (MIDDLE, 1, 1, 1), (MIDDLE, 1, 2, -1), (MIDDLE, 1, 2, 1),
    (MIDDLE, 1, 3, -1), (MIDDLE, 1, 3, 1), (COMBINE, 5, 5), (FAR, 2), (COMBINE, 5, 6),
    (COMBINE, 5, 7), (COMBINE, 4, 4), (COMBINE, 4, 5), (FULL, 2), (DGRAD, 0), (COMBINE, 4, 3),
    (HIDDEN, 0), (DERIVE,), (COMBINE, 5, 3), (COMBINE, 5, 4), (WGRAD, 0, 3), (COMBINE, 0, 15),
    (COMBINE, 1, 15), (COMBINE, 0, 13), (COMBINE, 0, 14), (COMBINE, 1, 14), (WGRAD, 0, 2),
    (COMBINE, 1, 13), (COMBINE, 0, 10), (WGRAD, 0, 1), (COMBINE, 1, 10), (WGRAD, 0, 0),
    (COMBINE, 5, 1), (COMBINE, 5, 2), (WGRAD, 1, 3), (COMBINE, 4, 1), (COMBINE, 2, 15),
    (COMBINE, 3, 15), (COMBINE, 2, 13), (COMBINE, 2, 14), (COMBINE, 3, 14), (WGRAD, 1, 2),
    (COMBINE, 4, 2), (COMBINE, 3, 13), (COMBINE, 2, 10), (WGRAD, 1, 1), (COMBINE, 0, 11),
    (COMBINE, 0, 12), (COMBINE, 1, 12), (COMBINE, 3, 10), (WGRAD, 1, 0), (COMBINE, 1, 11),
    (COMBINE, 0, 7), (COMBINE, 1, 8), (COMBINE, 1, 9), (SUMMED, 1, 0), (SUMMED, 1, 1),
    (SUMMED, 1, 2), (SUMMED, 1, 3), (BACK, 0), (COMBINE, 0, 6), (COMBINE, 0, 8), (COMBINE, 0, 9),
    (COMBINE, 1, 6), (COMBINE, 1, 7), (BACK, 1), (COMBINE, 2, 12), (COMBINE, 0, 3),
    (COMBINE, 0, 4), (COMBINE, 1, 3), (COMBINE, 1, 4), (BACK, 2), (COMBINE, 5, 0),
    (COMBINE, 3, 9), (START, 2, 0), (BACK, 3), (COMBINE, 2, 11), (COMBINE, 3, 11),
    (COMBINE, 3, 12), (COMBINE, 4, 0), (COMBINE, 2, 7), (COMBINE, 3, 8), (START, 2, 1), (LATE,),
    (COMBINE, 2, 6), (COMBINE, 2, 9), (COMBINE, 3, 6), (COMBINE, 3, 7), (START, 2, 2),
    (COMBINE, 2, 8), (COMBINE, 2, 3), (COMBINE, 2, 4), (START, 2, 3), (MIDDLE, 2, 0, -1),
    (MIDDLE, 2, 0, 1), (COMBINE, 0, 5), (COMBINE, 3, 4), (COMBINE, 1, 5), (COMBINE, 3, 3),
    (MIDDLE, 2, 1, -1), (MIDDLE, 2, 1, 1), (MIDDLE, 2, 2, -1), (MIDDLE, 2, 2, 1),
    (MIDDLE, 2, 3, -1), (MIDDLE, 2, 3, 1), (SUMMED, 2, 0), (SUMMED, 2, 1), (COMBINE, 3, 5),
    (COMBINE, 2, 5), (SUMMED, 2, 2), (SUMMED, 2, 3), (EARLY,), (COMBINE, 1, 1), (COMBINE, 0, 2),
    (COMBINE, 1, 2), (COMBINE, 0, 1), (COMBINE, 2, 2), (COMBINE, 3, 1), (COMBINE, 3, 2),
    (COMBINE, 2, 1), (COMBINE, 1, 0), (COMBINE, 0, 0), (COMBINE, 3, 0), (COMBINE, 2, 0),
]


def wrapped(n):
    n %= 4
    return n - 4 if n == 3 else n


def landing(hop):
    (da, db), ax, sg, _ = hop
    if ax == "a":
        da -= sg
    else:
        db -= sg
    return (wrapped(db), wrapped(da))


LANDS = [ORDER.index(landing(hop)) for hop in HOPS]
ARRIVALS = {o: [i for i, k in enumerate(LANDS) if ORDER[k] == o] for o in ORDER}
DUTIES = {o: [i for i, hop in enumerate(HOPS) if hop[0] == o] for o in ORDER}
PIECES = 2
DEEP = 128 // PIECES
HALF = DEEP // 2
SLOT, ARRIVED, GAINS, _at = {}, {}, {}, 0
for _k, _o in enumerate(ORDER):
    if DUTIES[_o]:
        GAINS[_k] = len(GAINS)
        _first = _at
        for _i in DUTIES[_o]:
            SLOT[_i] = _at
            _at += DEEP if HOPS[_i][3] is None else HALF
        ARRIVED[_k] = (_first, _at - _first)
ARRIVED_ROWS = _at
STRAIGHT_SUMS = ((0, 3),)
STRAIGHT_BLOCKS = (5,)


def scoped(f):
    return f


def turned(h, k):
    return ORDER.index(ORDER[k][::-1]) if h % 2 else k


def rows_of(h, k, part):
    start = turned(h, k) * 128 + h * DEEP
    return (start, DEEP) if part is None else (start + HALF * part, HALF)


def last_last(a, b):
    return lax.dot_general(a, b, (((1,), (1,)), ((), ())), preferred_element_type=F32)


def first_first(a, b):
    return lax.dot_general(a, b, (((0,), (0,)), ((), ())), preferred_element_type=F32)


def kernel(
    late_in, early_in, early_grad, pre_gain, post_gain, gate_w, up_w, down_w,
    gate_sum, up_sum, down_sum,
    late_out, early_out, gate_out, up_out, down_out,
    late_o, early_o, gate_o, up_o, down_o,
    late_v, early_v, grad_v, pre_v, post_v, gsum_v, usum_v, dsum_v,
    w_all, tok, tok_t, pre, dgate, dup, hid, part, pair, both, fwd, last, cot, hcot,
    gcot, ucot, grads, arrived, mixed, weighted,
    ag_s, ag_r, rs_s, rs_r, xa_s, xa_r, xr_s, xr_r, in_s,
):
    fs = lax.axis_index("fs")
    tp = lax.axis_index("tp")
    y, z = fs % 4, fs // 4
    par = (y + z) % 2
    core, x = tp % 2, tp // 2
    grad_scale = 1.0 / math.sqrt(8192.0)

    def fs_at(da, db):
        dy = (1 - par) * da + par * db
        dz = (1 - par) * db + par * da
        return ((z + dz + 4) % 4) * 4 + (y + dy + 4) % 4

    def torus(h, ax, sg):
        return (fs_at(sg, 0) if (ax == "a") == (h % 2 == 0) else fs_at(0, sg), tp)

    ring = {sg: (fs, ((x + sg + 4) % 4) * 2 + core) for sg in (1, -1, 2)}
    partner = (fs, x * 2 + 1 - core)
    columns = [pl.multiple_of(fs_at(*o) * 128, 128) for o in ORDER]

    fetched = []

    def fetch(src, dst):
        copy = pltpu.make_async_copy(src, dst, in_s.at[len(fetched)])
        copy.start()
        fetched.append(copy)
        return copy

    barrier = pltpu.get_barrier_semaphore()
    peers = [partner, ring[1], ring[-1], ring[2]] + [torus(0, ax, sg) for ax in "ab" for sg in (1, -1)]
    for peer in peers:
        pl.semaphore_signal(barrier, inc=1, device_id=peer, device_id_type=MESH)
    fetch_weights = [fetch(gate_w, w_all.at[0, pl.ds(0, 128)])]
    fetch_tokens = {1: fetch(early_in, early_v)}
    fetch_small = [fetch(pre_gain, pre_v)]
    fetch_weights.append(fetch(up_w, w_all.at[1, pl.ds(0, 128)]))
    fetch_tokens[0] = fetch(late_in, late_v)
    fetch_weights.append(fetch(down_w, w_all.at[2, pl.ds(0, 128)]))
    fetch_tokens[2] = fetch(early_grad, grad_v)
    fetch_small.append(fetch(post_gain, post_v))
    fetch_sums = [fetch(gate_sum, gsum_v), fetch(up_sum, usum_v), fetch(down_sum, dsum_v)]
    sums = ((gsum_v, gate_o, gate_out), (usum_v, up_o, up_out), (dsum_v, down_o, down_out))
    pl.semaphore_wait(barrier, len(peers))

    def send(src, dst, ss, rs, to):
        pltpu.make_async_remote_copy(
            src_ref=src, dst_ref=dst, send_sem=ss, recv_sem=rs,
            device_id=to, device_id_type=MESH,
        ).start()

    def arrive(dst, ss, rs):
        pltpu.make_async_remote_copy(
            src_ref=dst, dst_ref=dst, send_sem=ss, recv_sem=rs,
            device_id=partner, device_id_type=MESH,
        ).wait_recv()

    def pass_on(p, k):
        w, h = divmod(p, PIECES)
        for i in DUTIES[ORDER[k]]:
            _, ax, sg, q = HOPS[i]
            start, n = rows_of(h, k, q)
            there, _ = rows_of(h, LANDS[i], q)
            send(
                w_all.at[w, pl.ds(start, n)], w_all.at[w, pl.ds(there, n)],
                ag_s.at[p], ag_r.at[p, LANDS[i] - 1], torus(h, ax, sg),
            )

    @scoped
    def relay(p, k):
        w, h = divmod(p, PIECES)
        start, n = rows_of(h, k, None)
        arrive(w_all.at[w, pl.ds(start, n)], ag_s.at[p], ag_r.at[p, k - 1])
        pass_on(p, k)

    @scoped
    def own(p):
        if p % PIECES == 0:
            fetch_weights[p // PIECES].wait()
        pass_on(p, 0)

    def rows(j, row, n):
        if j < 2:
            return tok.at[j, pl.ds(row, n)]
        return cot.at[pl.ds(row, n), pl.ds(512 * (j - 2), 512)]

    def move(j, i, row, there, n, to):
        send(rows(j, row, n), rows(j, there, n), xa_s.at[j], xa_r.at[j, i], to)

    def come(j, i, row, n):
        arrive(rows(j, row, n), xa_s.at[j], xa_r.at[j, i])

    @scoped
    def spread(j):
        if j in STRAIGHT_BLOCKS:
            move(j, 2, 0, 128, 64, ring[2])
        move(j, 0, 0, 192, 64, ring[1])
        move(j, 1, 0, 64, 64, ring[-1])
        move(j, 3, 0, 256, 64, partner)

    @scoped
    def near(j, sg):
        at, there, part_at = (192, 128, 192) if sg == 1 else (64, 160, 96)
        come(j, (1 - sg) // 2, at, 64)
        if j not in STRAIGHT_BLOCKS:
            move(j, 2, part_at, there, 32, ring[sg])
        move(j, 3, at, 256 + at, 64, partner)

    @scoped
    def far(j):
        come(j, 2, 128, 64)
        move(j, 3, 128, 384, 64, partner)

    @scoped
    def full(j):
        come(j, 3, 256, 256)

    def pass_sum(v, g, i, row, n, ref, there, to):
        s = 4 * v + g
        send(
            both.at[v, g, pl.ds(row, n)], ref.at[v, g, pl.ds(there, n)],
            xr_s.at[s], xr_r.at[s, i], to,
        )

    def get_sum(v, g, i, ref, row, n):
        s = 4 * v + g
        arrive(ref.at[v, g, pl.ds(row, n)], xr_s.at[s], xr_r.at[s, i])

    def sum_pair(v, g):
        s = 4 * v + g
        send(part.at[v, g, pl.ds(256, 256)], pair.at[v, g], xr_s.at[s], xr_r.at[s, 0], partner)

    @scoped
    def start(v, g):
        get_sum(v, g, 0, pair, 0, 256)
        for r in (128, 64, 192, 0):
            both[v, g, r : r + 64] = (
                part[v, g, r : r + 64].astype(F32) + pair[v, g, r : r + 64].astype(F32)
            ).astype(BF)
            if r == 128 and (v, g) not in STRAIGHT_SUMS:
                pass_sum(v, g, 1, 128, 32, fwd, 0, ring[1])
                pass_sum(v, g, 2, 160, 32, fwd, 32, ring[-1])
            if (v, g) in STRAIGHT_SUMS and r:
                i, to = {128: (0, 2), 64: (1, 1), 192: (2, -1)}[r]
                pass_sum(v, g, 3, r, 64, last, 64 * i, ring[to])

    @scoped
    def middle(v, g, sg):
        i, r, t = (0, 64, 64) if sg == 1 else (1, 192, 224)
        get_sum(v, g, 1 + i, fwd, 32 * i, 32)
        both[v, g, t : t + 32] = (
            both[v, g, t : t + 32].astype(F32) + fwd[v, g, 32 * i : 32 * i + 32].astype(F32)
        ).astype(BF)
        pass_sum(v, g, 3, r, 64, last, 64 * i, ring[sg])

    @scoped
    def summed(v, g):
        n = 3 if (v, g) in STRAIGHT_SUMS else 2
        get_sum(v, g, 3, last, 0, 64 * n)
        total = both[v, g, :64].astype(F32)
        for i in range(n):
            total += last[v, g, 64 * i : 64 * i + 64].astype(F32)
        mixed[v, :, pl.ds(512 * g, 512)] = total.astype(BF)

    @scoped
    def combine(p, k):
        w, h = divmod(p, PIECES)
        if k in GAINS:
            first, n = ARRIVED[k]
            arrive(arrived.at[p, pl.ds(first, n)], rs_s.at[p], rs_r.at[p, GAINS[k]])
        for q in (0, 1):
            terms = []
            for i in DUTIES[ORDER[k]]:
                if HOPS[i][3] is None:
                    terms.append(SLOT[i] + HALF * q)
                elif HOPS[i][3] == q:
                    terms.append(SLOT[i])
            if terms:
                r, _ = rows_of(h, k, q)
                total = grads[w, r : r + HALF].astype(F32)
                for at in terms:
                    total += arrived[p, at : at + HALF].astype(F32)
                if k == 0:
                    olds, out, _ = sums[w]
                    out[r : r + HALF] = olds[r : r + HALF] + grad_scale * total
                else:
                    grads[w, r : r + HALF] = total.astype(BF)
        if k == 0:
            at = pl.ds(h * DEEP, DEEP)
            fetch(sums[w][1].at[at], sums[w][2].at[at])
        for i in ARRIVALS[ORDER[k]]:
            _, ax, sg, q = HOPS[i]
            r, n = rows_of(h, k, q)
            send(
                grads.at[w, pl.ds(r, n)], arrived.at[p, pl.ds(SLOT[i], n)],
                rs_s.at[p], rs_r.at[p, GAINS[ORDER.index(HOPS[i][0])]], torus(h, "b" if ax == "a" else "a", -sg),
            )

    def tiles(count, body):
        lax.fori_loop(0, count, lambda i, c: (body(i), c)[1], 0)

    @scoped
    def norm(m):
        if m == 1:
            fetch_small[0].wait()
        fetch_tokens[m].wait()
        source = (late_v, early_v)[m]
        values = source[...].astype(F32)
        inverse = lax.rsqrt(jnp.mean(values * values, axis=-1, keepdims=True) + NORM_EPS)
        for k, at in enumerate(columns):
            tok[m, 0:64, 128 * k : 128 * k + 128] = (
                source[:, pl.ds(at, 128)].astype(F32) * inverse * pre_v[:, pl.ds(at, 128)]
            ).astype(BF)

    @scoped
    def weigh():
        fetch_tokens[2].wait()
        fetch_small[1].wait()
        for copy in fetch_sums:
            copy.wait()
        for k, at in enumerate(columns):
            weighted[:, 128 * k : 128 * k + 128] = (
                0.5 * grad_v[:, pl.ds(at, 128)].astype(F32) * post_v[:, pl.ds(at, 128)]
            )

    @scoped
    def gate(m, t):
        r = 128 * t
        pre[m, r : r + 128] = jnp.dot(tok[m, r : r + 128], w_all[0], preferred_element_type=F32)

    @scoped
    def up(m, t):
        at = slice(128 * t, 128 * t + 128)
        ups = jnp.dot(tok[m, at], w_all[1], preferred_element_type=F32)
        gates = pre[m, at]
        s = jax.nn.sigmoid(gates)
        hid[m, at] = (gates * s * ups).astype(BF)
        if m == 1:
            dgate[at] = ups * s * (1.0 + gates * (1.0 - s))
            dup[at] = gates * s

    @scoped
    def down(v, g):
        def body(i):
            r = pl.multiple_of(256 - i * 256, 256)
            part[v, g, pl.ds(r, 256)] = last_last(
                hid[1 - v, pl.ds(r, 256)], w_all[2, pl.ds(512 * g, 512)]
            ).astype(BF)

        tiles(2, body)
        sum_pair(v, g)

    @scoped
    def back(g):
        def body(i):
            r = pl.multiple_of(i * 256, 256)
            part[2, g, pl.ds(r, 256)] = (
                last_last(gcot[pl.ds(r, 256)], w_all[0, pl.ds(512 * g, 512)])
                + last_last(ucot[pl.ds(r, 256)], w_all[1, pl.ds(512 * g, 512)])
            ).astype(BF)

        tiles(2, body)
        sum_pair(2, g)

    @scoped
    def cotangent():
        values = mixed[0].astype(F32)
        inverse = lax.rsqrt(jnp.mean(values * values, axis=-1, keepdims=True) + NORM_EPS)
        scaled = inverse**3 * jnp.mean(weighted[...] * values, axis=-1, keepdims=True)
        for g in (3, 2, 1, 0):
            at = slice(512 * g, 512 * g + 512)
            cot[0:64, at] = (
                inverse * weighted[:, at] - mixed[0, :, at].astype(F32) * scaled
            ).astype(BF)

    @scoped
    def hidden(g):
        def body(i):
            r = pl.multiple_of(i * 256, 256)
            term = jnp.dot(
                cot[pl.ds(r, 256), pl.ds(512 * g, 512)],
                w_all[2, pl.ds(512 * g, 512)],
                preferred_element_type=F32,
            )
            hcot[pl.ds(r, 256)] = hcot[pl.ds(r, 256)] + term if begun else term

        tiles(2, body)
        begun.append(g)

    @scoped
    def dgrad(g):
        grads[2, pl.ds(512 * g, 512)] = first_first(
            cot[:, pl.ds(512 * g, 512)], hid[1]
        ).astype(BF)

    @scoped
    def turn():
        for k in range(16):
            tok_t[128 * k : 128 * k + 128] = tok[1, :, 128 * k : 128 * k + 128].T

    @scoped
    def derive():
        gcot[...] = (hcot[...] * dgate[...]).astype(BF)
        ucot[...] = (hcot[...] * dup[...]).astype(BF)

    @scoped
    def wgrad(w, g):
        def body(i):
            r = pl.multiple_of(512 * g + i * 256, 256)
            grads[w, pl.ds(r, 256)] = jnp.dot(
                tok_t[pl.ds(r, 256)], (gcot, ucot)[w][...], preferred_element_type=F32
            ).astype(BF)

        tiles(2, body)

    @scoped
    def late_end():
        values = mixed[1].astype(F32)
        inverse = lax.rsqrt(jnp.mean(values * values, axis=-1, keepdims=True) + NORM_EPS)
        for k, at in enumerate(columns):
            late_o[:, pl.ds(at, 128)] = (
                late_v[:, pl.ds(at, 128)].astype(F32)
                + 0.5
                * mixed[1, :, 128 * k : 128 * k + 128].astype(F32)
                * inverse
                * post_v[:, pl.ds(at, 128)]
            ).astype(BF)
        fetch(late_o, late_out)

    @scoped
    def early_end():
        early = early_v[...].astype(F32)
        inverse = lax.rsqrt(jnp.mean(early * early, axis=-1, keepdims=True) + NORM_EPS)
        dots = jnp.zeros((64, 128), F32)
        for k, at in enumerate(columns):
            dots += (
                mixed[2, :, 128 * k : 128 * k + 128].astype(F32)
                * pre_v[:, pl.ds(at, 128)]
                * early_v[:, pl.ds(at, 128)].astype(F32)
            )
        slope = inverse**3 * (jnp.sum(dots, axis=-1, keepdims=True) * (1.0 / 2048.0))
        for k, at in enumerate(columns):
            early_o[:, pl.ds(at, 128)] = (
                grad_v[:, pl.ds(at, 128)].astype(F32)
                + inverse
                * (mixed[2, :, 128 * k : 128 * k + 128].astype(F32) * pre_v[:, pl.ds(at, 128)])
                - early_v[:, pl.ds(at, 128)].astype(F32) * slope
            ).astype(BF)
        fetch(early_o, early_out)

    begun = []
    steps = (
        own, relay, norm, spread, near, far, full, weigh, gate, up, down, back, start, middle,
        summed, turn, cotangent, hidden, dgrad, derive, wgrad, combine, late_end, early_end,
    )
    for name, *at in SCRIPT:
        steps[name](*at)

    def leave(ref, ss):
        pltpu.make_async_remote_copy(
            src_ref=ref, dst_ref=ref, send_sem=ss, recv_sem=ss,
            device_id=partner, device_id_type=MESH,
        ).wait_send()

    for p in range(3 * PIECES):
        leave(w_all.at[p // PIECES, pl.ds(0, 15 * DEEP)], ag_s.at[p])
        leave(grads.at[p // PIECES, pl.ds(0, 15 * DEEP)], rs_s.at[p])
    for j in range(6):
        leave(rows(j, 0, 448), xa_s.at[j])
    for s in range(12):
        leave(part.at[s // 4, s % 4, pl.ds(0, 448)], xr_s.at[s])
    for copy in fetched[11:]:
        copy.wait()


def hand_over(*refs):
    sources, targets, held, (in_s, out_s) = refs[:5], refs[5:10], refs[10:15], refs[15:]
    copies = [pltpu.make_async_copy(sources[i], held[i], in_s.at[i]) for i in range(5)]
    for copy in copies:
        copy.start()
    for i in range(5):
        copies[i].wait()
        copies[i] = pltpu.make_async_copy(held[i], targets[i], out_s.at[i])
        copies[i].start()
    for copy in copies:
        copy.wait()


def per_device(
    late_input,
    early_input,
    early_grad,
    pre_gain,
    post_gain,
    gate_weight,
    up_weight,
    down_weight,
    gate_sum,
    up_sum,
    down_gradient_sum,
):
    sem = pltpu.SemaphoreType.DMA
    vmem = pltpu.VMEM
    tokens = jax.ShapeDtypeStruct((64, 2048), BF)
    total = jax.ShapeDtypeStruct((128, 512), F32)
    results = pl.pallas_call(
        kernel,
        name="half_step",
        out_shape=(tokens, tokens, total, total, total),
        in_specs=[pl.BlockSpec(memory_space=pl.ANY)] * 11,
        out_specs=[pl.BlockSpec(memory_space=pl.ANY)] * 5,
        scratch_shapes=[
            vmem((64, 2048), BF),
            vmem((64, 2048), BF),
            vmem((128, 512), F32),
            vmem((128, 512), F32),
            vmem((128, 512), F32),
            vmem((64, 2048), BF),
            vmem((64, 2048), BF),
            vmem((64, 2048), BF),
            vmem((1, 2048), F32),
            vmem((1, 2048), F32),
            vmem((128, 512), F32),
            vmem((128, 512), F32),
            vmem((128, 512), F32),
            vmem((3, 2048, 512), BF),
            vmem((2, 512, 2048), BF),
            vmem((2048, 512), BF),
            vmem((2, 512, 512), F32),
            vmem((512, 512), F32),
            vmem((512, 512), F32),
            vmem((2, 512, 512), BF),
            vmem((3, 4, 512, 512), BF),
            vmem((3, 4, 256, 512), BF),
            vmem((3, 4, 256, 512), BF),
            vmem((3, 4, 64, 512), BF),
            vmem((3, 4, 192, 512), BF),
            vmem((512, 2048), BF),
            vmem((512, 512), F32),
            vmem((512, 512), BF),
            vmem((512, 512), BF),
            vmem((3, 2048, 512), BF),
            vmem((3 * PIECES, ARRIVED_ROWS, 512), BF),
            vmem((3, 64, 2048), BF),
            vmem((64, 2048), F32),
            sem((3 * PIECES,)),
            sem((3 * PIECES, 15)),
            sem((3 * PIECES,)),
            sem((3 * PIECES, len(GAINS))),
            sem((6,)),
            sem((6, 4)),
            sem((12,)),
            sem((12, 4)),
            sem((13 + 3 * PIECES,)),
        ],
        compiler_params=pltpu.CompilerParams(
            collective_id=0, has_side_effects=True, vmem_limit_bytes=67043328
        ),
    )(
        late_input, early_input, early_grad, pre_gain.reshape(1, -1), post_gain.reshape(1, -1),
        gate_weight, up_weight, down_weight, gate_sum, up_sum, down_gradient_sum,
    )
    return pl.pallas_call(
        hand_over,
        name="hand_over",
        out_shape=(tokens, tokens, total, total, total),
        in_specs=[pl.BlockSpec(memory_space=pl.ANY)] * 5,
        out_specs=[pl.BlockSpec(memory_space=pl.ANY)] * 5,
        scratch_shapes=[
            vmem((64, 2048), BF),
            vmem((64, 2048), BF),
            vmem((128, 512), F32),
            vmem((128, 512), F32),
            vmem((128, 512), F32),
            sem((5,)),
            sem((5,)),
        ],
        compiler_params=pltpu.CompilerParams(vmem_limit_bytes=67043328),
    )(*results)


def solution(mesh):
    rows, both = P(("fs", "tp"), None), P("fs", "tp")
    return jax.shard_map(
        per_device,
        mesh=mesh,
        in_specs=(rows,) * 3 + (P(), P()) + (both,) * 6,
        out_specs=(rows, rows, both, both, both),
        check_vma=False,
    )
```

time: 315 us -> 107 us (0.34)
  waiting for transfers between devices: 196 us -> 0 us
  Pallas kernels: 0 us -> 106 us
  blocking collectives: 29.7 us -> 0 us
  matrix products: 27.9 us -> 0 us
  local copies, waits for them, and re-layouts: 27.4 us -> 0 us
  other arithmetic: 15.7 us -> 0 us
  between operations: 13.9 us -> 0.82 us
  starting transfers between devices: 3.91 us -> 0 us
    pallas_call x0 -> x2, Pallas kernels: none -> 106 us  [the longest x1 104 us: per_device(): pl.pallas_call(kernel, name='half_step', out_shape=(tokens, tokens, total...]
    all_gather x2 -> x0, waiting for transfers between devices: 96.3 us -> none  [the longest x1 63.5 us: sent_together(): lax.all_gather(both, axis, axis=dim, tiled=True)]
    unnamed x5 -> x0, waiting for transfers between devices: 39.1 us -> none
    reduce_scatter x1 -> x0, waiting for transfers between devices: 36.9 us -> none  [per_device(): lax.psum_scatter(gated_product.reshape(lax.axis_size('tp') * tok_rows, 2...]
    all_to_all x1 -> x0, blocking collectives: 29.7 us -> none  [sent_to_all(): lax.all_to_all(jnp.broadcast_to(shard[None], (peers, *shard.shape)), axis...]
    dot_general x9 -> x0, matrix products: 27.9 us -> none  [the longest x2 7.09 us: contract_last(): lax.dot_general(first_op, second_op, (((1,), (1,)), ((), ())), preferred_...]
    all_to_all x1 -> x0, waiting for transfers between devices: 23.5 us -> none  [summed_on_arrival(): lax.all_to_all(parts, axis, split_axis=0, concat_axis=0, tiled=True)]
    unnamed x39 -> x0, local copies, waits for them, and re-layouts: 17.1 us -> none
  transfers between devices with their start and end apart: 5 -> 0, of which waited for: 5 -> 0; matrix products, arithmetic and copies ran while one was open for 5% -> 0% of each run, Pallas kernels for 0% -> 0%
where the time goes in v2:
time: 107 us
  Pallas kernels  106 us (99%)
    pallas_call x1, Pallas kernels, per_device(): pl.pallas_call(kernel, name='half_step', out_shape=(tokens, tokens, total...  104 us

profile of v2, /device:TPU:0, one launch (start us, length us, event | category | flops | bytes accessed | tf_op | source)
XLA Modules:
  0.0 107.0 jit_solution(11343338789045054194)
XLA Ops:
  0.6 104.1 %half_step.1 = (bf16[64,2048]{1,0:T(8,128)(2,1)}, bf16[64,2048]{1,0:T(8,128)(2,1)}, f32[128,512]{1,0:T(8,128)}, f32[128,512]{1,0:T(8,128)}, f32[128,512]{1,0:T(8,128)}) custom-call(bf16[64,2048]{1,0:T(8,128)(2,1)} %late_in.1, bf16[64,2048]{1,0:T(8,128)(2,1)} %early_in.1, bf16[64,2048]{1,0:T(8,128)(2,1)} %early_grad.1, f32[1,2048]{1,0:T(1,128)} %bitcast.2, ...), custom_call_target="tpu_custom_call" | custom-call | tf_op jit(solution)/shard_map/half_step/pallas_call | solution.py:565
  104.7 2.1 %hand_over.1 = (bf16[64,2048]{1,0:T(8,128)(2,1)}, bf16[64,2048]{1,0:T(8,128)(2,1)}, f32[128,512]{1,0:T(8,128)}, f32[128,512]{1,0:T(8,128)}, f32[128,512]{1,0:T(8,128)}) custom-call(bf16[64,2048]{1,0:T(8,128)(2,1)} %get-tuple-element.10.refs_0_, bf16[64,2048]{1,0:T(8,128)(2,1)} %get-tuple-element.11.refs_1_, f32[128,512]{1,0:T(8,128)} %get-tuple-element.12.refs_2_, ...), custom_call_target="tpu_custom_call" | custom-call | tf_op jit(solution)/shard_map/hand_over/pallas_call | solution.py:622

commit v3 on v2

v3 whole, which is shorter than its diff:
```python
import math

import jax
import jax.numpy as jnp
from jax import lax
from jax.experimental import pallas as pl
from jax.experimental.pallas import tpu as pltpu
from jax.sharding import PartitionSpec as P

NORM_EPS = 1e-06
BF = jnp.bfloat16
F32 = jnp.float32
MESH = pl.DeviceIdType.MESH

ORDER = [
    (0, 0), (0, 1), (0, -1), (1, 0),
    (-1, 0), (2, 0), (1, 1), (1, -1),
    (-1, 1), (-1, -1), (0, 2), (1, 2),
    (-1, 2), (2, 1), (2, -1), (2, 2),
]
HOPS = (
    [((0, 0), ax, sg, None) for ax in "ab" for sg in (1, -1)]
    + [((2, 0), "b", sg, None) for sg in (1, -1)]
    + [((0, s), "a", sg, None) for s in (1, -1) for sg in (1, -1)]
    + [((0, s), "b", -s, (1 + s) // 2) for s in (1, -1)]
    + [((s, t), "b", -t, (1 + t) // 2) for s in (1, -1) for t in (1, -1)]
    + [((s, 0), "a", -s, (1 + s) // 2) for s in (1, -1)]
    + [((s, 2), "a", -s, (1 + s) // 2) for s in (1, -1)]
)


(
    OWN, RELAY, NORM, SPREAD, NEAR, FAR, FULL, WEIGH, GATE, UP, DOWN, BACK, START, MIDDLE,
    SUMMED, TURN, COT, HIDDEN, DGRAD, DERIVE, WGRAD, COMBINE, LATE, EARLY,
    PASS, GIVE,
) = range(26)
SCRIPT = [
    (NORM, 1), (SPREAD, 1), (OWN, 0), (PASS, 0, 0), (PASS, 0, 1), (PASS, 0, 2), (PASS, 0, 3),
    (OWN, 1), (NORM, 0), (PASS, 1, 0), (PASS, 1, 1), (PASS, 1, 2), (PASS, 1, 3), (OWN, 2),
    (SPREAD, 0), (WEIGH,), (PASS, 2, 0), (PASS, 2, 1), (PASS, 2, 2), (PASS, 2, 3), (PASS, 3, 2),
    (PASS, 3, 3), (PASS, 3, 0), (PASS, 3, 1), (RELAY, 0, 2), (RELAY, 0, 1), (RELAY, 0, 4),
    (RELAY, 0, 3), (PASS, 0, 6), (PASS, 0, 7), (PASS, 0, 11), (PASS, 0, 10), (PASS, 4, 2),
    (PASS, 4, 3), (RELAY, 1, 4), (RELAY, 1, 3), (RELAY, 1, 2), (RELAY, 1, 1), (PASS, 0, 8),
    (PASS, 0, 9), (PASS, 1, 6), (PASS, 1, 7), (RELAY, 2, 2), (RELAY, 2, 1), (RELAY, 2, 4),
    (RELAY, 2, 3), (PASS, 1, 11), (PASS, 1, 10), (PASS, 2, 6), (PASS, 2, 7), (PASS, 1, 8),
    (PASS, 1, 9), (NEAR, 1, -1), (NEAR, 1, 1), (RELAY, 3, 1), (RELAY, 3, 2), (RELAY, 3, 3),
    (RELAY, 3, 4), (RELAY, 0, 5), (PASS, 2, 8), (PASS, 2, 9), (PASS, 0, 4), (PASS, 0, 5),
    (RELAY, 0, 7), (RELAY, 0, 6), (PASS, 3, 11), (PASS, 3, 10), (PASS, 2, 11), (PASS, 2, 10),
    (RELAY, 0, 9), (RELAY, 0, 8), (PASS, 0, 17), (PASS, 0, 16), (PASS, 0, 13), (PASS, 0, 12),
    (RELAY, 1, 5), (RELAY, 1, 7), (RELAY, 1, 6), (PASS, 1, 4), (PASS, 1, 5), (PASS, 0, 15),
    (PASS, 0, 14), (PASS, 3, 6), (PASS, 3, 7), (RELAY, 2, 7), (RELAY, 2, 6), (RELAY, 1, 9),
    (RELAY, 1, 8), (PASS, 1, 13), (PASS, 1, 12), (NEAR, 0, -1), (NEAR, 0, 1), (PASS, 1, 15),
    (PASS, 1, 14), (PASS, 3, 8), (PASS, 3, 9), (RELAY, 2, 9), (RELAY, 2, 8), (RELAY, 0, 12),
    (RELAY, 0, 11), (PASS, 0, 19), (PASS, 0, 18), (RELAY, 3, 5), (RELAY, 2, 5), (PASS, 3, 4),
    (PASS, 3, 5), (PASS, 2, 4), (PASS, 2, 5), (RELAY, 0, 10), (RELAY, 0, 13), (FAR, 1),
    (RELAY, 0, 14), (PASS, 4, 0), (PASS, 4, 1), (PASS, 1, 17), (PASS, 1, 16), (RELAY, 4, 3),
    (RELAY, 4, 4), (RELAY, 1, 12), (RELAY, 1, 11), (PASS, 1, 19), (PASS, 1, 18), (RELAY, 1, 13),
    (RELAY, 3, 7), (RELAY, 3, 6), (FULL, 1), (TURN,), (PASS, 2, 12), (PASS, 2, 13), (PASS, 2, 16),
    (PASS, 2, 17), (RELAY, 1, 14), (PASS, 3, 13), (PASS, 3, 12), (PASS, 2, 15), (PASS, 2, 14),
    (FAR, 0), (RELAY, 0, 15), (RELAY, 3, 9), (RELAY, 3, 8), (PASS, 3, 15), (PASS, 3, 14),
    (PASS, 5, 0), (PASS, 5, 1), (PASS, 5, 2), (PASS, 5, 3), (RELAY, 3, 12), (RELAY, 3, 11),
    (RELAY, 2, 12), (RELAY, 2, 11), (FULL, 0), (PASS, 3, 19), (PASS, 3, 18), (RELAY, 1, 10),
    (PASS, 2, 19), (PASS, 2, 18), (PASS, 3, 17), (PASS, 3, 16), (RELAY, 4, 2), (RELAY, 4, 1),
    (RELAY, 1, 15), (GATE, 1, 0), (GATE, 1, 1), (PASS, 4, 10), (PASS, 4, 11), (PASS, 4, 6),
    (PASS, 4, 7), (RELAY, 2, 10), (RELAY, 2, 13), (GATE, 1, 2), (GATE, 1, 3), (RELAY, 2, 14),
    (RELAY, 3, 13), (GATE, 0, 0), (PASS, 4, 8), (PASS, 4, 9), (RELAY, 3, 14), (GATE, 0, 1),
    (GATE, 0, 2), (RELAY, 5, 1), (PASS, 5, 6), (PASS, 5, 7), (RELAY, 5, 2), (GATE, 0, 3),
    (PASS, 5, 10), (PASS, 5, 11), (PASS, 5, 8), (PASS, 5, 9), (RELAY, 3, 15), (RELAY, 5, 3),
    (RELAY, 5, 4), (PASS, 4, 17), (PASS, 4, 16), (RELAY, 2, 15), (RELAY, 3, 10), (UP, 1, 0),
    (UP, 1, 1), (PASS, 5, 16), (PASS, 5, 17), (RELAY, 4, 5), (UP, 1, 2), (PASS, 4, 4),
    (PASS, 4, 5), (RELAY, 4, 6), (RELAY, 4, 7), (UP, 1, 3), (DOWN, 0, 0), (PASS, 4, 12),
    (PASS, 4, 13), (UP, 0, 0), (RELAY, 4, 8), (RELAY, 4, 9), (RELAY, 5, 6), (PASS, 5, 12),
    (RELAY, 5, 7), (PASS, 5, 13), (UP, 0, 1), (PASS, 4, 14), (PASS, 4, 15), (RELAY, 5, 5),
    (PASS, 5, 4), (PASS, 5, 5), (UP, 0, 2), (RELAY, 4, 10), (UP, 0, 3), (RELAY, 5, 8),
    (PASS, 5, 14), (RELAY, 5, 9), (PASS, 5, 15), (START, 0, 0), (DOWN, 1, 0), (RELAY, 5, 10),
    (DOWN, 0, 1), (DOWN, 1, 1), (RELAY, 4, 11), (PASS, 4, 18), (RELAY, 4, 12), (PASS, 4, 19),
    (RELAY, 5, 13), (DOWN, 1, 2), (RELAY, 4, 13), (RELAY, 4, 14), (RELAY, 5, 11), (PASS, 5, 18),
    (RELAY, 5, 12), (PASS, 5, 19), (DOWN, 0, 3), (MIDDLE, 0, 0, -1), (MIDDLE, 0, 0, 1),
    (START, 0, 1), (RELAY, 5, 14), (DOWN, 0, 2), (START, 0, 3), (RELAY, 4, 15), (START, 0, 2),
    (RELAY, 5, 15), (DOWN, 0, 4), (DOWN, 1, 3), (SUMMED, 0, 0), (START, 0, 4), (MIDDLE, 0, 1, -1),
    (MIDDLE, 0, 1, 1), (MIDDLE, 0, 2, 1), (MIDDLE, 0, 2, -1), (SUMMED, 0, 3), (SUMMED, 0, 4),
    (SUMMED, 0, 1), (SUMMED, 0, 2), (COT,), (SPREAD, 2), (SPREAD, 3), (NEAR, 2, -1), (NEAR, 2, 1),
    (SPREAD, 4), (NEAR, 3, 1), (NEAR, 3, -1), (SPREAD, 5), (FAR, 2), (FULL, 2), (DGRAD, 0),
    (GIVE, 4, 18), (GIVE, 4, 19), (GIVE, 5, 18), (GIVE, 5, 19), (FAR, 3), (NEAR, 4, 1),
    (NEAR, 4, -1), (SPREAD, 6), (FULL, 3), (DGRAD, 1), (GIVE, 4, 12), (GIVE, 4, 13),
    (GIVE, 4, 14), (GIVE, 4, 15), (NEAR, 5, 1), (NEAR, 5, -1), (START, 1, 0), (START, 1, 1),
    (START, 1, 2), (START, 1, 3), (COMBINE, 5, 11), (GIVE, 5, 5), (COMBINE, 5, 12), (GIVE, 5, 4),
    (FAR, 4), (FULL, 4), (DGRAD, 2), (GIVE, 5, 12), (GIVE, 5, 13), (GIVE, 5, 14), (GIVE, 5, 15),
    (NEAR, 6, -1), (NEAR, 6, 1), (COMBINE, 4, 11), (GIVE, 4, 5), (COMBINE, 4, 12), (GIVE, 4, 4),
    (COMBINE, 4, 9), (HIDDEN, 3), (GIVE, 4, 16), (GIVE, 4, 17), (FAR, 5), (COMBINE, 5, 5),
    (GIVE, 5, 10), (GIVE, 5, 11), (MIDDLE, 1, 0, 1), (MIDDLE, 1, 0, -1), (GIVE, 4, 8),
    (MIDDLE, 1, 1, 1), (MIDDLE, 1, 1, -1), (FULL, 5), (DGRAD, 3), (GIVE, 5, 16), (GIVE, 5, 17),
    (COMBINE, 4, 6), (GIVE, 4, 7), (COMBINE, 4, 7), (COMBINE, 4, 8), (MIDDLE, 1, 2, -1),
    (MIDDLE, 1, 2, 1), (HIDDEN, 2), (GIVE, 4, 6), (GIVE, 4, 9), (COMBINE, 5, 6), (GIVE, 5, 7),
    (COMBINE, 5, 7), (GIVE, 5, 6), (MIDDLE, 1, 3, -1), (MIDDLE, 1, 3, 1), (COMBINE, 5, 8),
    (GIVE, 5, 9), (COMBINE, 5, 9), (GIVE, 5, 8), (COMBINE, 4, 5), (FAR, 6), (GIVE, 4, 10),
    (GIVE, 4, 11), (FULL, 6), (DGRAD, 4), (COMBINE, 4, 3), (GIVE, 4, 3), (COMBINE, 4, 4),
    (GIVE, 4, 2), (COMBINE, 5, 3), (GIVE, 5, 3), (COMBINE, 5, 4), (GIVE, 5, 2), (HIDDEN, 0),
    (HIDDEN, 1), (COMBINE, 5, 1), (GIVE, 5, 1), (DERIVE,), (WGRAD, 0, 3), (GIVE, 0, 18),
    (GIVE, 0, 19), (GIVE, 1, 19), (GIVE, 0, 13), (GIVE, 1, 14), (GIVE, 1, 15), (WGRAD, 0, 2),
    (GIVE, 1, 18), (GIVE, 0, 15), (GIVE, 1, 12), (GIVE, 1, 13), (COMBINE, 5, 2), (WGRAD, 0, 1),
    (GIVE, 0, 12), (GIVE, 0, 16), (GIVE, 0, 17), (GIVE, 1, 17), (COMBINE, 4, 1), (COMBINE, 4, 2),
    (WGRAD, 0, 0), (GIVE, 0, 14), (GIVE, 4, 0), (GIVE, 4, 1), (GIVE, 5, 0), (WGRAD, 1, 3),
    (GIVE, 3, 18), (WGRAD, 1, 2), (GIVE, 2, 18), (GIVE, 2, 19), (GIVE, 3, 19), (GIVE, 2, 12),
    (COMBINE, 0, 11), (COMBINE, 0, 12), (COMBINE, 1, 12), (WGRAD, 1, 1), (GIVE, 0, 4),
    (GIVE, 0, 5), (GIVE, 1, 4), (GIVE, 3, 12), (COMBINE, 0, 7), (COMBINE, 1, 8), (COMBINE, 1, 9),
    (WGRAD, 1, 0), (GIVE, 3, 14), (COMBINE, 0, 9), (COMBINE, 1, 11), (COMBINE, 1, 6),
    (COMBINE, 1, 7), (SUMMED, 1, 0), (SUMMED, 1, 1), (SUMMED, 1, 2), (SUMMED, 1, 3), (BACK, 0),
    (GIVE, 1, 5), (GIVE, 2, 13), (GIVE, 2, 14), (GIVE, 3, 13), (GIVE, 1, 16), (COMBINE, 0, 3),
    (COMBINE, 0, 4), (COMBINE, 0, 6), (COMBINE, 0, 8), (GIVE, 2, 15), (GIVE, 3, 15),
    (COMBINE, 1, 4), (BACK, 1), (GIVE, 2, 16), (GIVE, 2, 17), (GIVE, 3, 16), (GIVE, 3, 17),
    (COMBINE, 3, 11), (BACK, 2), (GIVE, 3, 5), (GIVE, 0, 6), (GIVE, 1, 6), (GIVE, 1, 7),
    (COMBINE, 2, 11), (COMBINE, 2, 12), (COMBINE, 2, 6), (COMBINE, 3, 12), (START, 2, 0),
    (BACK, 3), (GIVE, 2, 4), (GIVE, 2, 5), (GIVE, 3, 4), (GIVE, 0, 7), (COMBINE, 0, 5),
    (COMBINE, 3, 6), (COMBINE, 3, 8), (START, 2, 1), (COMBINE, 4, 0), (COMBINE, 5, 0), (LATE,),
    (COMBINE, 2, 7), (COMBINE, 2, 8), (COMBINE, 3, 7), (START, 2, 2), (GIVE, 0, 10),
    (COMBINE, 1, 3), (GIVE, 0, 9), (GIVE, 0, 8), (GIVE, 0, 11), (COMBINE, 1, 5), (COMBINE, 2, 9),
    (COMBINE, 3, 9), (GIVE, 1, 9), (START, 2, 3), (COMBINE, 3, 3), (GIVE, 1, 8), (COMBINE, 2, 3),
    (COMBINE, 2, 4), (COMBINE, 3, 4), (MIDDLE, 2, 0, -1), (MIDDLE, 2, 0, 1), (GIVE, 1, 10),
    (GIVE, 1, 11), (GIVE, 3, 7), (GIVE, 2, 7), (GIVE, 2, 6), (GIVE, 3, 6), (MIDDLE, 2, 1, -1),
    (MIDDLE, 2, 1, 1), (MIDDLE, 2, 2, -1), (MIDDLE, 2, 2, 1), (GIVE, 3, 9), (GIVE, 2, 9),
    (GIVE, 2, 8), (GIVE, 3, 8), (COMBINE, 3, 5), (COMBINE, 2, 5), (MIDDLE, 2, 3, -1),
    (MIDDLE, 2, 3, 1), (COMBINE, 0, 1), (GIVE, 2, 10), (GIVE, 3, 10), (GIVE, 3, 11),
    (GIVE, 2, 11), (COMBINE, 0, 2), (SUMMED, 2, 0), (GIVE, 0, 3), (GIVE, 0, 1), (GIVE, 0, 0),
    (GIVE, 0, 2), (COMBINE, 1, 1), (COMBINE, 1, 2), (SUMMED, 2, 1), (GIVE, 1, 1), (GIVE, 1, 3),
    (GIVE, 1, 2), (GIVE, 1, 0), (SUMMED, 2, 2), (GIVE, 2, 3), (GIVE, 3, 3), (GIVE, 3, 2),
    (GIVE, 2, 2), (COMBINE, 2, 1), (COMBINE, 3, 1), (COMBINE, 2, 2), (COMBINE, 3, 2),
    (SUMMED, 2, 3), (EARLY,), (GIVE, 2, 0), (GIVE, 2, 1), (GIVE, 3, 0), (GIVE, 3, 1),
    (COMBINE, 0, 0), (COMBINE, 1, 0), (COMBINE, 2, 0), (COMBINE, 3, 0),
]


def wrapped(n):
    n %= 4
    return n - 4 if n == 3 else n


def landing(hop):
    (da, db), ax, sg, _ = hop
    if ax == "a":
        da -= sg
    else:
        db -= sg
    return (wrapped(db), wrapped(da))


LANDS = [ORDER.index(landing(hop)) for hop in HOPS]
ARRIVALS = {o: [i for i, k in enumerate(LANDS) if ORDER[k] == o] for o in ORDER}
DUTIES = {o: [i for i, hop in enumerate(HOPS) if hop[0] == o] for o in ORDER}
PIECES = 2
DEEP = 128 // PIECES
HALF = DEEP // 2
SLOT, ARRIVED, GAINS, _at = {}, {}, {}, 0
for _k, _o in enumerate(ORDER):
    if DUTIES[_o]:
        GAINS[_k] = len(GAINS)
        _first = _at
        for _i in DUTIES[_o]:
            SLOT[_i] = _at
            _at += DEEP if HOPS[_i][3] is None else HALF
        ARRIVED[_k] = (_first, _at - _first)
ARRIVED_ROWS = _at
STRAIGHT_SUMS = ((0, 3), (0, 4))
STRAIGHT_BLOCKS = (2, 3)
SUMS = (
    ((0, 5), (5, 4), (9, 4), (13, 2), (15, 1)),
    ((0, 4), (4, 4), (8, 4), (12, 4)),
    ((0, 4), (4, 4), (8, 4), (12, 4)),
)
BLOCKS = ((15, 1), (13, 2), (9, 4), (5, 4), (0, 5))
SUM_AT = (0, len(SUMS[0]), len(SUMS[0]) + len(SUMS[1]))


def lanes(group):
    return pl.ds(128 * group[0], 128 * group[1])


def scoped(f):
    return f


def turned(h, k):
    return ORDER.index(ORDER[k][::-1]) if h % 2 else k


def rows_of(h, k, part):
    start = turned(h, k) * 128 + h * DEEP
    return (start, DEEP) if part is None else (start + HALF * part, HALF)


def last_last(a, b):
    return lax.dot_general(a, b, (((1,), (1,)), ((), ())), preferred_element_type=F32)


def first_first(a, b):
    return lax.dot_general(a, b, (((0,), (0,)), ((), ())), preferred_element_type=F32)


def kernel(
    late_in, early_in, early_grad, pre_gain, post_gain, gate_w, up_w, down_w,
    gate_sum, up_sum, down_sum,
    late_out, early_out, gate_out, up_out, down_out,
    late_v, early_v, grad_v, pre_v, post_v, gsum_v, usum_v, dsum_v,
    w_all, tok, tok_t, pre, dgate, dup, hid, part, pair, both, fwd, last, cot, hcot,
    gcot, ucot, grads, arrived, mixed, weighted,
    ag_s, ag_r, rs_s, rs_r, xa_s, xa_r, xr_s, xr_r, in_s,
):
    fs = lax.axis_index("fs")
    tp = lax.axis_index("tp")
    y, z = fs % 4, fs // 4
    par = (y + z) % 2
    core, x = tp % 2, tp // 2
    grad_scale = 1.0 / math.sqrt(8192.0)

    def fs_at(da, db):
        dy = (1 - par) * da + par * db
        dz = (1 - par) * db + par * da
        return ((z + dz + 4) % 4) * 4 + (y + dy + 4) % 4

    def torus(h, ax, sg):
        return (fs_at(sg, 0) if (ax == "a") == (h % 2 == 0) else fs_at(0, sg), tp)

    ring = {sg: (fs, ((x + sg + 4) % 4) * 2 + core) for sg in (1, -1, 2)}
    partner = (fs, x * 2 + 1 - core)
    columns = [pl.multiple_of(fs_at(*o) * 128, 128) for o in ORDER]

    fetched = []

    def fetch(src, dst):
        copy = pltpu.make_async_copy(src, dst, in_s.at[len(fetched)])
        copy.start()
        fetched.append(copy)
        return copy

    barrier = pltpu.get_barrier_semaphore()
    peers = [partner, ring[1], ring[-1], ring[2]] + [torus(0, ax, sg) for ax in "ab" for sg in (1, -1)]
    for peer in peers:
        pl.semaphore_signal(barrier, inc=1, device_id=peer, device_id_type=MESH)
    fetch_weights = [fetch(gate_w, w_all.at[0, pl.ds(0, 128)])]
    fetch_tokens = {1: fetch(early_in, early_v)}
    fetch_small = [fetch(pre_gain, pre_v)]
    fetch_weights.append(fetch(up_w, w_all.at[1, pl.ds(0, 128)]))
    fetch_tokens[0] = fetch(late_in, late_v)
    fetch_weights.append(fetch(down_w, w_all.at[2, pl.ds(0, 128)]))
    fetch_tokens[2] = fetch(early_grad, grad_v)
    fetch_small.append(fetch(post_gain, post_v))
    fetch_sums = [fetch(gate_sum, gsum_v), fetch(up_sum, usum_v), fetch(down_sum, dsum_v)]
    sums = ((gsum_v, gate_out), (usum_v, up_out), (dsum_v, down_out))
    pl.semaphore_wait(barrier, len(peers))

    def send(src, dst, ss, rs, to):
        pltpu.make_async_remote_copy(
            src_ref=src, dst_ref=dst, send_sem=ss, recv_sem=rs,
            device_id=to, device_id_type=MESH,
        ).start()

    def arrive(dst, ss, rs):
        pltpu.make_async_remote_copy(
            src_ref=dst, dst_ref=dst, send_sem=ss, recv_sem=rs,
            device_id=partner, device_id_type=MESH,
        ).wait_recv()

    @scoped
    def pass_on(p, i):
        w, h = divmod(p, PIECES)
        offset, ax, sg, q = HOPS[i]
        start, n = rows_of(h, ORDER.index(offset), q)
        there, _ = rows_of(h, LANDS[i], q)
        send(
            w_all.at[w, pl.ds(start, n)], w_all.at[w, pl.ds(there, n)],
            ag_s, ag_r.at[p, LANDS[i] - 1], torus(h, ax, sg),
        )

    @scoped
    def relay(p, k):
        w, h = divmod(p, PIECES)
        start, n = rows_of(h, k, None)
        arrive(w_all.at[w, pl.ds(start, n)], ag_s, ag_r.at[p, k - 1])

    @scoped
    def own(w):
        fetch_weights[w].wait()

    def rows(j, row, n):
        if j < 2:
            return tok.at[j, pl.ds(row, n)]
        return cot.at[pl.ds(row, n), lanes(BLOCKS[j - 2])]

    def move(j, i, row, there, n, to):
        send(rows(j, row, n), rows(j, there, n), xa_s.at[min(j // 2, 1)], xa_r.at[j, i], to)

    def come(j, i, row, n):
        arrive(rows(j, row, n), xa_s.at[min(j // 2, 1)], xa_r.at[j, i])

    @scoped
    def spread(j):
        move(j, 0, 0, 192, 64, ring[1])
        move(j, 1, 0, 64, 64, ring[-1])
        if j in STRAIGHT_BLOCKS:
            move(j, 2, 0, 128, 64, ring[2])
        move(j, 3, 0, 256, 64, partner)

    @scoped
    def near(j, sg):
        at, there, part_at = (192, 128, 192) if sg == 1 else (64, 160, 96)
        come(j, (1 - sg) // 2, at, 64)
        if j not in STRAIGHT_BLOCKS:
            move(j, 2, part_at, there, 32, ring[sg])
        move(j, 3, at, 256 + at, 64, partner)

    @scoped
    def far(j):
        come(j, 2, 128, 64)
        move(j, 3, 128, 384, 64, partner)

    @scoped
    def full(j):
        come(j, 3, 256, 256)

    def pass_sum(v, g, i, source, row, n, ref, there, to):
        at = lanes(SUMS[v][g])
        send(
            source.at[v, pl.ds(row, n), at], ref.at[v, pl.ds(there, n), at],
            xr_s, xr_r.at[SUM_AT[v] + g, i], to,
        )

    def get_sum(v, g, i, ref, row, n):
        arrive(ref.at[v, pl.ds(row, n), lanes(SUMS[v][g])], xr_s, xr_r.at[SUM_AT[v] + g, i])

    @scoped
    def start(v, g):
        at = lanes(SUMS[v][g])
        get_sum(v, g, 0, pair, 0, 256)
        for r in (64, 192, 128, 0):
            if r == 64 and (v, g) not in STRAIGHT_SUMS:
                r = 128
            elif r == 128 and (v, g) not in STRAIGHT_SUMS:
                r = 64
            both[v, r : r + 64, at] = (
                part[v, r : r + 64, at].astype(F32) + pair[v, r : r + 64, at].astype(F32)
            ).astype(BF)
            if (v, g) in STRAIGHT_SUMS and r:
                i, to = {128: (0, 2), 64: (1, 1), 192: (2, -1)}[r]
                pass_sum(v, g, 3, both, r, 64, last, 64 * i, ring[to])
            elif r == 128:
                pass_sum(v, g, 1, both, 128, 32, fwd, 0, ring[1])
                pass_sum(v, g, 2, both, 160, 32, fwd, 32, ring[-1])

    @scoped
    def middle(v, g, sg):
        at = lanes(SUMS[v][g])
        i, r, t = (0, 64, 64) if sg == 1 else (1, 192, 224)
        get_sum(v, g, 1 + i, fwd, 32 * i, 32)
        both[v, t : t + 32, at] = (
            both[v, t : t + 32, at].astype(F32) + fwd[v, 32 * i : 32 * i + 32, at].astype(F32)
        ).astype(BF)
        pass_sum(v, g, 3, both, r, 64, last, 64 * i, ring[sg])

    @scoped
    def summed(v, g):
        at = lanes(SUMS[v][g])
        n = 3 if (v, g) in STRAIGHT_SUMS else 2
        get_sum(v, g, 3, last, 0, 64 * n)
        total = both[v, :64, at].astype(F32)
        for i in range(n):
            total += last[v, 64 * i : 64 * i + 64, at].astype(F32)
        mixed[v, :, at] = total.astype(BF)

    @scoped
    def combine(p, k):
        w, h = divmod(p, PIECES)
        if k in GAINS:
            first, n = ARRIVED[k]
            arrive(arrived.at[p, pl.ds(first, n)], rs_s, rs_r.at[p, GAINS[k]])
        for q in (0, 1):
            terms = []
            for i in DUTIES[ORDER[k]]:
                if HOPS[i][3] is None:
                    terms.append(SLOT[i] + HALF * q)
                elif HOPS[i][3] == q:
                    terms.append(SLOT[i])
            if terms:
                r, _ = rows_of(h, k, q)
                total = grads[w, r : r + HALF].astype(F32)
                for at in terms:
                    total += arrived[p, at : at + HALF].astype(F32)
                if k == 0:
                    olds, out = sums[w]
                    out[r : r + HALF] = olds[r : r + HALF] + grad_scale * total
                else:
                    grads[w, r : r + HALF] = total.astype(BF)

    @scoped
    def give(p, i):
        w, h = divmod(p, PIECES)
        offset, ax, sg, q = HOPS[i]
        r, n = rows_of(h, LANDS[i], q)
        send(
            grads.at[w, pl.ds(r, n)], arrived.at[p, pl.ds(SLOT[i], n)],
            rs_s, rs_r.at[p, GAINS[ORDER.index(offset)]],
            torus(h, "b" if ax == "a" else "a", -sg),
        )

    def tiles(count, body):
        lax.fori_loop(0, count, lambda i, c: (body(i), c)[1], 0)

    @scoped
    def norm(m):
        if m == 1:
            fetch_small[0].wait()
        fetch_tokens[m].wait()
        source = (late_v, early_v)[m]
        values = source[...].astype(F32)
        inverse = lax.rsqrt(jnp.mean(values * values, axis=-1, keepdims=True) + NORM_EPS)
        for k, at in enumerate(columns):
            tok[m, 0:64, 128 * k : 128 * k + 128] = (
                source[:, pl.ds(at, 128)].astype(F32) * inverse * pre_v[:, pl.ds(at, 128)]
            ).astype(BF)

    @scoped
    def weigh():
        fetch_tokens[2].wait()
        fetch_small[1].wait()
        for copy in fetch_sums:
            copy.wait()
        for k, at in enumerate(columns):
            weighted[:, 128 * k : 128 * k + 128] = (
                0.5 * grad_v[:, pl.ds(at, 128)].astype(F32) * post_v[:, pl.ds(at, 128)]
            )

    @scoped
    def gate(m, t):
        r = 128 * t
        pre[m, r : r + 128] = jnp.dot(tok[m, r : r + 128], w_all[0], preferred_element_type=F32)

    @scoped
    def up(m, t):
        at = slice(128 * t, 128 * t + 128)
        ups = jnp.dot(tok[m, at], w_all[1], preferred_element_type=F32)
        gates = pre[m, at]
        s = jax.nn.sigmoid(gates)
        hid[m, at] = (gates * s * ups).astype(BF)
        if m == 1:
            dgate[at] = ups * s * (1.0 + gates * (1.0 - s))
            dup[at] = gates * s

    @scoped
    def down(v, g):
        first, n = SUMS[v][g]

        def body(i):
            r = pl.multiple_of(256 - i * 256, 256)
            part[v, pl.ds(r, 256), lanes(SUMS[v][g])] = last_last(
                hid[1 - v, pl.ds(r, 256)], w_all[2, pl.ds(128 * first, 128 * n)]
            ).astype(BF)

        tiles(2, body)
        pass_sum(v, g, 0, part, 256, 256, pair, 0, partner)

    @scoped
    def back(g):
        first, n = SUMS[2][g]

        def body(i):
            r = pl.multiple_of(i * 256, 256)
            part[2, pl.ds(r, 256), lanes(SUMS[2][g])] = (
                last_last(gcot[pl.ds(r, 256)], w_all[0, pl.ds(128 * first, 128 * n)])
                + last_last(ucot[pl.ds(r, 256)], w_all[1, pl.ds(128 * first, 128 * n)])
            ).astype(BF)

        tiles(2, body)
        pass_sum(2, g, 0, part, 256, 256, pair, 0, partner)

    @scoped
    def cotangent():
        values = mixed[0].astype(F32)
        inverse = lax.rsqrt(jnp.mean(values * values, axis=-1, keepdims=True) + NORM_EPS)
        scaled = inverse**3 * jnp.mean(weighted[...] * values, axis=-1, keepdims=True)
        for g in (3, 2, 1, 0):
            at = slice(512 * g, 512 * g + 512)
            cot[0:64, at] = (
                inverse * weighted[:, at] - mixed[0, :, at].astype(F32) * scaled
            ).astype(BF)

    @scoped
    def hidden(g):
        def body(i):
            r = pl.multiple_of(i * 256, 256)
            term = jnp.dot(
                cot[pl.ds(r, 256), pl.ds(512 * g, 512)],
                w_all[2, pl.ds(512 * g, 512)],
                preferred_element_type=F32,
            )
            hcot[pl.ds(r, 256)] = hcot[pl.ds(r, 256)] + term if begun else term

        tiles(2, body)
        begun.append(g)

    @scoped
    def dgrad(g):
        first, n = BLOCKS[g]
        grads[2, pl.ds(128 * first, 128 * n)] = first_first(
            cot[:, lanes(BLOCKS[g])], hid[1]
        ).astype(BF)

    @scoped
    def turn():
        for k in range(16):
            tok_t[128 * k : 128 * k + 128] = tok[1, :, 128 * k : 128 * k + 128].T

    @scoped
    def derive():
        gcot[...] = (hcot[...] * dgate[...]).astype(BF)
        ucot[...] = (hcot[...] * dup[...]).astype(BF)

    @scoped
    def wgrad(w, g):
        def body(i):
            r = pl.multiple_of(512 * g + i * 256, 256)
            grads[w, pl.ds(r, 256)] = jnp.dot(
                tok_t[pl.ds(r, 256)], (gcot, ucot)[w][...], preferred_element_type=F32
            ).astype(BF)

        tiles(2, body)

    @scoped
    def late_end():
        values = mixed[1].astype(F32)
        inverse = lax.rsqrt(jnp.mean(values * values, axis=-1, keepdims=True) + NORM_EPS)
        for k, at in enumerate(columns):
            late_out[:, pl.ds(at, 128)] = (
                late_v[:, pl.ds(at, 128)].astype(F32)
                + 0.5
                * mixed[1, :, 128 * k : 128 * k + 128].astype(F32)
                * inverse
                * post_v[:, pl.ds(at, 128)]
            ).astype(BF)

    @scoped
    def early_end():
        early = early_v[...].astype(F32)
        inverse = lax.rsqrt(jnp.mean(early * early, axis=-1, keepdims=True) + NORM_EPS)
        dots = jnp.zeros((64, 128), F32)
        for k, at in enumerate(columns):
            dots += (
                mixed[2, :, 128 * k : 128 * k + 128].astype(F32)
                * pre_v[:, pl.ds(at, 128)]
                * early_v[:, pl.ds(at, 128)].astype(F32)
            )
        slope = inverse**3 * (jnp.sum(dots, axis=-1, keepdims=True) * (1.0 / 2048.0))
        for k, at in enumerate(columns):
            early_out[:, pl.ds(at, 128)] = (
                grad_v[:, pl.ds(at, 128)].astype(F32)
                + inverse
                * (mixed[2, :, 128 * k : 128 * k + 128].astype(F32) * pre_v[:, pl.ds(at, 128)])
                - early_v[:, pl.ds(at, 128)].astype(F32) * slope
            ).astype(BF)

    begun = []
    steps = (
        own, relay, norm, spread, near, far, full, weigh, gate, up, down, back, start, middle,
        summed, turn, cotangent, hidden, dgrad, derive, wgrad, combine, late_end, early_end,
        pass_on, give,
    )
    for name, *at in SCRIPT:
        steps[name](*at)

    def leave(ref, ss):
        pltpu.make_async_remote_copy(
            src_ref=ref, dst_ref=ref, send_sem=ss, recv_sem=ss,
            device_id=partner, device_id_type=MESH,
        ).wait_send()

    leave(w_all.reshape(3 * 2048, 512).at[pl.ds(0, 3 * 15 * 128)], ag_s)
    leave(grads.reshape(3 * 2048, 512).at[pl.ds(0, 3 * 15 * 128)], rs_s)
    leave(tok.reshape(1024, 2048).at[pl.ds(0, 2 * 448)], xa_s.at[0])
    leave(cot.at[pl.ds(0, 448)], xa_s.at[1])
    leave(part.reshape(3 * 512, 2048).at[pl.ds(0, 3 * 448)], xr_s)


def hand_over(*refs):
    copies = [pltpu.make_async_copy(refs[i], refs[5 + i], refs[10].at[i]) for i in range(5)]
    for copy in copies:
        copy.start()
    for copy in copies:
        copy.wait()


def per_device(
    late_input,
    early_input,
    early_grad,
    pre_gain,
    post_gain,
    gate_weight,
    up_weight,
    down_weight,
    gate_sum,
    up_sum,
    down_gradient_sum,
):
    sem = pltpu.SemaphoreType.DMA
    vmem = pltpu.VMEM
    tokens = jax.ShapeDtypeStruct((64, 2048), BF)
    total = jax.ShapeDtypeStruct((128, 512), F32)
    results = pl.pallas_call(
        kernel,
        name="half_step",
        out_shape=(vmem((64, 2048), BF),) * 2 + (vmem((128, 512), F32),) * 3,
        in_specs=[pl.BlockSpec(memory_space=pl.ANY)] * 11,
        out_specs=[pl.BlockSpec(memory_space=vmem)] * 5,
        scratch_shapes=[
            vmem((64, 2048), BF),
            vmem((64, 2048), BF),
            vmem((64, 2048), BF),
            vmem((1, 2048), F32),
            vmem((1, 2048), F32),
            vmem((128, 512), F32),
            vmem((128, 512), F32),
            vmem((128, 512), F32),
            vmem((3, 2048, 512), BF),
            vmem((2, 512, 2048), BF),
            vmem((2048, 512), BF),
            vmem((2, 512, 512), F32),
            vmem((512, 512), F32),
            vmem((512, 512), F32),
            vmem((2, 512, 512), BF),
            vmem((3, 512, 2048), BF),
            vmem((3, 256, 2048), BF),
            vmem((3, 256, 2048), BF),
            vmem((3, 64, 2048), BF),
            vmem((3, 192, 2048), BF),
            vmem((512, 2048), BF),
            vmem((512, 512), F32),
            vmem((512, 512), BF),
            vmem((512, 512), BF),
            vmem((3, 2048, 512), BF),
            vmem((3 * PIECES, ARRIVED_ROWS, 512), BF),
            vmem((3, 64, 2048), BF),
            vmem((64, 2048), F32),
            sem,
            sem((3 * PIECES, 15)),
            sem,
            sem((3 * PIECES, len(GAINS))),
            sem((2,)),
            sem((2 + len(BLOCKS), 4)),
            sem,
            sem((SUM_AT[2] + len(SUMS[2]), 4)),
            sem((11,)),
        ],
        compiler_params=pltpu.CompilerParams(
            collective_id=0, has_side_effects=True, vmem_limit_bytes=60 * 2**20
        ),
    )(
        late_input, early_input, early_grad, pre_gain.reshape(1, -1), post_gain.reshape(1, -1),
        gate_weight, up_weight, down_weight, gate_sum, up_sum, down_gradient_sum,
    )
    return pl.pallas_call(
        hand_over,
        name="hand_over",
        out_shape=(tokens, tokens, total, total, total),
        in_specs=[pl.BlockSpec(memory_space=vmem)] * 5,
        out_specs=[pl.BlockSpec(memory_space=pl.ANY)] * 5,
        scratch_shapes=[sem((5,))],
        compiler_params=pltpu.CompilerParams(vmem_limit_bytes=4 * 2**20),
    )(*results)


def solution(mesh):
    rows, both = P(("fs", "tp"), None), P("fs", "tp")
    return jax.shard_map(
        per_device,
        mesh=mesh,
        in_specs=(rows,) * 3 + (P(), P()) + (both,) * 6,
        out_specs=(rows, rows, both, both, both),
        check_vma=False,
    )
```

time: 107 us -> 103 us (0.963)
  Pallas kernels: 106 us -> 102 us
    pallas_call x1, Pallas kernels: 104 us -> 100 us  [per_device(): pl.pallas_call(kernel, name='half_step', out_shape=(vmem((64, 2048), BF),...]
where the time goes in v3:
time: 103 us; the launch traced here: 102 us
  Pallas kernels  102 us (99%)
    pallas_call x1, Pallas kernels, per_device(): pl.pallas_call(kernel, name='half_step', out_shape=(vmem((64, 2048), BF),...  100 us

profile of v3, /device:TPU:0, one launch (start us, length us, event | category | flops | bytes accessed | tf_op | source)
XLA Modules:
  0.0 102.4 jit_solution(15208091690622193810)
XLA Ops:
  0.6 100.5 %half_step.1 = (bf16[64,2048]{1,0:T(8,128)(2,1)S(1)}, bf16[64,2048]{1,0:T(8,128)(2,1)S(1)}, f32[128,512]{1,0:T(8,128)S(1)}, f32[128,512]{1,0:T(8,128)S(1)}, f32[128,512]{1,0:T(8,128)S(1)}) custom-call(bf16[64,2048]{1,0:T(8,128)(2,1)} %late_in.1, bf16[64,2048]{1,0:T(8,128)(2,1)} %early_in.1, bf16[64,2048]{1,0:T(8,128)(2,1)} %early_grad.1, f32[1,2048]{1,0:T(1,128)} %bitcast.2, ...), custom_call_target="tpu_custom_call" | custom-call | tf_op jit(solution)/shard_map/half_step/pallas_call | solution.py:606
  101.1 1.1 %hand_over.1 = (bf16[64,2048]{1,0:T(8,128)(2,1)}, bf16[64,2048]{1,0:T(8,128)(2,1)}, f32[128,512]{1,0:T(8,128)}, f32[128,512]{1,0:T(8,128)}, f32[128,512]{1,0:T(8,128)}) custom-call(bf16[64,2048]{1,0:T(8,128)(2,1)S(1)} %get-tuple-element.10.refs_0_, bf16[64,2048]{1,0:T(8,128)(2,1)S(1)} %get-tuple-element.11.refs_1_, ...), custom_call_target="tpu_custom_call" | custom-call | tf_op jit(solution)/shard_map/hand_over/pallas_call | solution.py:658

commit v4 on v3

--- a/solution.py
+++ b/solution.py
@@ -36,38 +36,38 @@
 ) = range(26)
 SCRIPT = [
     (NORM, 1), (SPREAD, 1), (OWN, 0), (PASS, 0, 0), (PASS, 0, 1), (PASS, 0, 2), (PASS, 0, 3),
-    (OWN, 1), (NORM, 0), (PASS, 1, 0), (PASS, 1, 1), (PASS, 1, 2), (PASS, 1, 3), (OWN, 2),
+    (NORM, 0), (PASS, 1, 0), (PASS, 1, 1), (PASS, 1, 2), (PASS, 1, 3), (OWN, 1), (OWN, 2),
     (SPREAD, 0), (WEIGH,), (PASS, 2, 0), (PASS, 2, 1), (PASS, 2, 2), (PASS, 2, 3), (PASS, 3, 2),
     (PASS, 3, 3), (PASS, 3, 0), (PASS, 3, 1), (RELAY, 0, 2), (RELAY, 0, 1), (RELAY, 0, 4),
     (RELAY, 0, 3), (PASS, 0, 6), (PASS, 0, 7), (PASS, 0, 11), (PASS, 0, 10), (PASS, 4, 2),
-    (PASS, 4, 3), (RELAY, 1, 4), (RELAY, 1, 3), (RELAY, 1, 2), (RELAY, 1, 1), (PASS, 0, 8),
-    (PASS, 0, 9), (PASS, 1, 6), (PASS, 1, 7), (RELAY, 2, 2), (RELAY, 2, 1), (RELAY, 2, 4),
-    (RELAY, 2, 3), (PASS, 1, 11), (PASS, 1, 10), (PASS, 2, 6), (PASS, 2, 7), (PASS, 1, 8),
-    (PASS, 1, 9), (NEAR, 1, -1), (NEAR, 1, 1), (RELAY, 3, 1), (RELAY, 3, 2), (RELAY, 3, 3),
-    (RELAY, 3, 4), (RELAY, 0, 5), (PASS, 2, 8), (PASS, 2, 9), (PASS, 0, 4), (PASS, 0, 5),
-    (RELAY, 0, 7), (RELAY, 0, 6), (PASS, 3, 11), (PASS, 3, 10), (PASS, 2, 11), (PASS, 2, 10),
-    (RELAY, 0, 9), (RELAY, 0, 8), (PASS, 0, 17), (PASS, 0, 16), (PASS, 0, 13), (PASS, 0, 12),
-    (RELAY, 1, 5), (RELAY, 1, 7), (RELAY, 1, 6), (PASS, 1, 4), (PASS, 1, 5), (PASS, 0, 15),
-    (PASS, 0, 14), (PASS, 3, 6), (PASS, 3, 7), (RELAY, 2, 7), (RELAY, 2, 6), (RELAY, 1, 9),
-    (RELAY, 1, 8), (PASS, 1, 13), (PASS, 1, 12), (NEAR, 0, -1), (NEAR, 0, 1), (PASS, 1, 15),
-    (PASS, 1, 14), (PASS, 3, 8), (PASS, 3, 9), (RELAY, 2, 9), (RELAY, 2, 8), (RELAY, 0, 12),
-    (RELAY, 0, 11), (PASS, 0, 19), (PASS, 0, 18), (RELAY, 3, 5), (RELAY, 2, 5), (PASS, 3, 4),
-    (PASS, 3, 5), (PASS, 2, 4), (PASS, 2, 5), (RELAY, 0, 10), (RELAY, 0, 13), (FAR, 1),
-    (RELAY, 0, 14), (PASS, 4, 0), (PASS, 4, 1), (PASS, 1, 17), (PASS, 1, 16), (RELAY, 4, 3),
-    (RELAY, 4, 4), (RELAY, 1, 12), (RELAY, 1, 11), (PASS, 1, 19), (PASS, 1, 18), (RELAY, 1, 13),
-    (RELAY, 3, 7), (RELAY, 3, 6), (FULL, 1), (TURN,), (PASS, 2, 12), (PASS, 2, 13), (PASS, 2, 16),
-    (PASS, 2, 17), (RELAY, 1, 14), (PASS, 3, 13), (PASS, 3, 12), (PASS, 2, 15), (PASS, 2, 14),
-    (FAR, 0), (RELAY, 0, 15), (RELAY, 3, 9), (RELAY, 3, 8), (PASS, 3, 15), (PASS, 3, 14),
-    (PASS, 5, 0), (PASS, 5, 1), (PASS, 5, 2), (PASS, 5, 3), (RELAY, 3, 12), (RELAY, 3, 11),
-    (RELAY, 2, 12), (RELAY, 2, 11), (FULL, 0), (PASS, 3, 19), (PASS, 3, 18), (RELAY, 1, 10),
-    (PASS, 2, 19), (PASS, 2, 18), (PASS, 3, 17), (PASS, 3, 16), (RELAY, 4, 2), (RELAY, 4, 1),
-    (RELAY, 1, 15), (GATE, 1, 0), (GATE, 1, 1), (PASS, 4, 10), (PASS, 4, 11), (PASS, 4, 6),
-    (PASS, 4, 7), (RELAY, 2, 10), (RELAY, 2, 13), (GATE, 1, 2), (GATE, 1, 3), (RELAY, 2, 14),
-    (RELAY, 3, 13), (GATE, 0, 0), (PASS, 4, 8), (PASS, 4, 9), (RELAY, 3, 14), (GATE, 0, 1),
-    (GATE, 0, 2), (RELAY, 5, 1), (PASS, 5, 6), (PASS, 5, 7), (RELAY, 5, 2), (GATE, 0, 3),
-    (PASS, 5, 10), (PASS, 5, 11), (PASS, 5, 8), (PASS, 5, 9), (RELAY, 3, 15), (RELAY, 5, 3),
-    (RELAY, 5, 4), (PASS, 4, 17), (PASS, 4, 16), (RELAY, 2, 15), (RELAY, 3, 10), (UP, 1, 0),
-    (UP, 1, 1), (PASS, 5, 16), (PASS, 5, 17), (RELAY, 4, 5), (UP, 1, 2), (PASS, 4, 4),
+    (PASS, 4, 3), (RELAY, 1, 4), (RELAY, 1, 3), (RELAY, 1, 2), (RELAY, 1, 1), (PASS, 1, 11),
+    (PASS, 1, 10), (PASS, 0, 8), (PASS, 0, 9), (PASS, 1, 6), (PASS, 1, 7), (RELAY, 2, 2),
+    (RELAY, 2, 1), (RELAY, 2, 4), (RELAY, 2, 3), (PASS, 2, 6), (PASS, 2, 7), (PASS, 2, 11),
+    (PASS, 2, 10), (NEAR, 1, 1), (NEAR, 1, -1), (RELAY, 3, 1), (RELAY, 3, 2), (RELAY, 3, 3),
+    (RELAY, 3, 4), (PASS, 1, 8), (PASS, 1, 9), (RELAY, 0, 5), (PASS, 3, 11), (PASS, 3, 10),
+    (RELAY, 0, 7), (RELAY, 0, 6), (PASS, 2, 8), (PASS, 2, 9), (PASS, 0, 4), (PASS, 0, 5),
+    (RELAY, 1, 5), (PASS, 1, 4), (PASS, 1, 5), (PASS, 0, 13), (PASS, 0, 12), (RELAY, 0, 9),
+    (RELAY, 0, 8), (RELAY, 1, 7), (RELAY, 1, 6), (PASS, 0, 15), (PASS, 0, 14), (RELAY, 2, 5),
+    (PASS, 0, 17), (PASS, 0, 16), (PASS, 2, 4), (PASS, 2, 5), (RELAY, 2, 7), (RELAY, 2, 6),
+    (PASS, 1, 13), (PASS, 1, 12), (NEAR, 0, 1), (NEAR, 0, -1), (RELAY, 1, 8), (RELAY, 1, 9),
+    (RELAY, 3, 5), (PASS, 1, 15), (PASS, 1, 14), (PASS, 3, 6), (PASS, 3, 7), (PASS, 3, 4),
+    (PASS, 3, 5), (RELAY, 2, 9), (RELAY, 2, 8), (RELAY, 0, 12), (RELAY, 0, 11), (PASS, 3, 8),
+    (PASS, 3, 9), (RELAY, 0, 13), (PASS, 0, 19), (PASS, 0, 18), (FAR, 1), (RELAY, 1, 12),
+    (RELAY, 1, 11), (RELAY, 0, 14), (PASS, 4, 0), (PASS, 4, 1), (PASS, 1, 19), (PASS, 1, 18),
+    (RELAY, 4, 3), (RELAY, 4, 4), (RELAY, 0, 10), (PASS, 1, 17), (PASS, 1, 16), (RELAY, 1, 13),
+    (RELAY, 2, 12), (RELAY, 2, 11), (FULL, 1), (TURN,), (PASS, 2, 18), (PASS, 2, 19),
+    (PASS, 2, 12), (PASS, 2, 13), (RELAY, 1, 14), (PASS, 2, 17), (PASS, 2, 16), (PASS, 2, 15),
+    (PASS, 2, 14), (FAR, 0), (RELAY, 3, 7), (RELAY, 3, 6), (PASS, 5, 2), (PASS, 5, 3),
+    (PASS, 5, 0), (PASS, 5, 1), (RELAY, 3, 12), (RELAY, 3, 11), (RELAY, 0, 15), (RELAY, 3, 9),
+    (RELAY, 3, 8), (FULL, 0), (PASS, 3, 13), (PASS, 3, 12), (PASS, 3, 19), (PASS, 3, 18),
+    (RELAY, 1, 15), (PASS, 3, 15), (PASS, 3, 14), (PASS, 3, 17), (PASS, 3, 16), (RELAY, 4, 2),
+    (RELAY, 4, 1), (RELAY, 1, 10), (GATE, 1, 0), (GATE, 1, 1), (PASS, 4, 10), (PASS, 4, 11),
+    (PASS, 4, 6), (PASS, 4, 7), (RELAY, 2, 13), (RELAY, 2, 15), (GATE, 1, 2), (GATE, 1, 3),
+    (RELAY, 2, 10), (RELAY, 2, 14), (GATE, 0, 0), (PASS, 4, 8), (PASS, 4, 9), (GATE, 0, 1),
+    (GATE, 0, 2), (RELAY, 5, 1), (PASS, 5, 6), (PASS, 5, 7), (RELAY, 5, 2), (RELAY, 5, 3),
+    (RELAY, 5, 4), (GATE, 0, 3), (PASS, 5, 10), (PASS, 5, 11), (PASS, 5, 8), (PASS, 5, 9),
+    (RELAY, 3, 13), (RELAY, 3, 15), (PASS, 4, 17), (PASS, 4, 16), (RELAY, 3, 14), (RELAY, 3, 10),
+    (UP, 1, 0), (UP, 1, 1), (PASS, 5, 16), (PASS, 5, 17), (RELAY, 4, 5), (UP, 1, 2), (PASS, 4, 4),
     (PASS, 4, 5), (RELAY, 4, 6), (RELAY, 4, 7), (UP, 1, 3), (DOWN, 0, 0), (PASS, 4, 12),
     (PASS, 4, 13), (UP, 0, 0), (RELAY, 4, 8), (RELAY, 4, 9), (RELAY, 5, 6), (PASS, 5, 12),
     (RELAY, 5, 7), (PASS, 5, 13), (UP, 0, 1), (PASS, 4, 14), (PASS, 4, 15), (RELAY, 5, 5),
@@ -75,58 +75,57 @@
     (PASS, 5, 14), (RELAY, 5, 9), (PASS, 5, 15), (START, 0, 0), (DOWN, 1, 0), (RELAY, 5, 10),
     (DOWN, 0, 1), (DOWN, 1, 1), (RELAY, 4, 11), (PASS, 4, 18), (RELAY, 4, 12), (PASS, 4, 19),
     (RELAY, 5, 13), (DOWN, 1, 2), (RELAY, 4, 13), (RELAY, 4, 14), (RELAY, 5, 11), (PASS, 5, 18),
-    (RELAY, 5, 12), (PASS, 5, 19), (DOWN, 0, 3), (MIDDLE, 0, 0, -1), (MIDDLE, 0, 0, 1),
+    (RELAY, 5, 12), (PASS, 5, 19), (DOWN, 0, 3), (MIDDLE, 0, 0, 1), (MIDDLE, 0, 0, -1),
     (START, 0, 1), (RELAY, 5, 14), (DOWN, 0, 2), (START, 0, 3), (RELAY, 4, 15), (START, 0, 2),
-    (RELAY, 5, 15), (DOWN, 0, 4), (DOWN, 1, 3), (SUMMED, 0, 0), (START, 0, 4), (MIDDLE, 0, 1, -1),
-    (MIDDLE, 0, 1, 1), (MIDDLE, 0, 2, 1), (MIDDLE, 0, 2, -1), (SUMMED, 0, 3), (SUMMED, 0, 4),
-    (SUMMED, 0, 1), (SUMMED, 0, 2), (COT,), (SPREAD, 2), (SPREAD, 3), (NEAR, 2, -1), (NEAR, 2, 1),
+    (RELAY, 5, 15), (DOWN, 0, 4), (DOWN, 1, 3), (SUMMED, 0, 0), (START, 0, 4), (MIDDLE, 0, 1, 1),
+    (MIDDLE, 0, 1, -1), (MIDDLE, 0, 2, 1), (MIDDLE, 0, 2, -1), (SUMMED, 0, 3), (SUMMED, 0, 4),
+    (SUMMED, 0, 1), (SUMMED, 0, 2), (COT,), (SPREAD, 2), (SPREAD, 3), (NEAR, 2, 1), (NEAR, 2, -1),
     (SPREAD, 4), (NEAR, 3, 1), (NEAR, 3, -1), (SPREAD, 5), (FAR, 2), (FULL, 2), (DGRAD, 0),
     (GIVE, 4, 18), (GIVE, 4, 19), (GIVE, 5, 18), (GIVE, 5, 19), (FAR, 3), (NEAR, 4, 1),
     (NEAR, 4, -1), (SPREAD, 6), (FULL, 3), (DGRAD, 1), (GIVE, 4, 12), (GIVE, 4, 13),
-    (GIVE, 4, 14), (GIVE, 4, 15), (NEAR, 5, 1), (NEAR, 5, -1), (START, 1, 0), (START, 1, 1),
-    (START, 1, 2), (START, 1, 3), (COMBINE, 5, 11), (GIVE, 5, 5), (COMBINE, 5, 12), (GIVE, 5, 4),
-    (FAR, 4), (FULL, 4), (DGRAD, 2), (GIVE, 5, 12), (GIVE, 5, 13), (GIVE, 5, 14), (GIVE, 5, 15),
-    (NEAR, 6, -1), (NEAR, 6, 1), (COMBINE, 4, 11), (GIVE, 4, 5), (COMBINE, 4, 12), (GIVE, 4, 4),
-    (COMBINE, 4, 9), (HIDDEN, 3), (GIVE, 4, 16), (GIVE, 4, 17), (FAR, 5), (COMBINE, 5, 5),
-    (GIVE, 5, 10), (GIVE, 5, 11), (MIDDLE, 1, 0, 1), (MIDDLE, 1, 0, -1), (GIVE, 4, 8),
-    (MIDDLE, 1, 1, 1), (MIDDLE, 1, 1, -1), (FULL, 5), (DGRAD, 3), (GIVE, 5, 16), (GIVE, 5, 17),
-    (COMBINE, 4, 6), (GIVE, 4, 7), (COMBINE, 4, 7), (COMBINE, 4, 8), (MIDDLE, 1, 2, -1),
-    (MIDDLE, 1, 2, 1), (HIDDEN, 2), (GIVE, 4, 6), (GIVE, 4, 9), (COMBINE, 5, 6), (GIVE, 5, 7),
-    (COMBINE, 5, 7), (GIVE, 5, 6), (MIDDLE, 1, 3, -1), (MIDDLE, 1, 3, 1), (COMBINE, 5, 8),
-    (GIVE, 5, 9), (COMBINE, 5, 9), (GIVE, 5, 8), (COMBINE, 4, 5), (FAR, 6), (GIVE, 4, 10),
-    (GIVE, 4, 11), (FULL, 6), (DGRAD, 4), (COMBINE, 4, 3), (GIVE, 4, 3), (COMBINE, 4, 4),
-    (GIVE, 4, 2), (COMBINE, 5, 3), (GIVE, 5, 3), (COMBINE, 5, 4), (GIVE, 5, 2), (HIDDEN, 0),
-    (HIDDEN, 1), (COMBINE, 5, 1), (GIVE, 5, 1), (DERIVE,), (WGRAD, 0, 3), (GIVE, 0, 18),
-    (GIVE, 0, 19), (GIVE, 1, 19), (GIVE, 0, 13), (GIVE, 1, 14), (GIVE, 1, 15), (WGRAD, 0, 2),
-    (GIVE, 1, 18), (GIVE, 0, 15), (GIVE, 1, 12), (GIVE, 1, 13), (COMBINE, 5, 2), (WGRAD, 0, 1),
-    (GIVE, 0, 12), (GIVE, 0, 16), (GIVE, 0, 17), (GIVE, 1, 17), (COMBINE, 4, 1), (COMBINE, 4, 2),
-    (WGRAD, 0, 0), (GIVE, 0, 14), (GIVE, 4, 0), (GIVE, 4, 1), (GIVE, 5, 0), (WGRAD, 1, 3),
-    (GIVE, 3, 18), (WGRAD, 1, 2), (GIVE, 2, 18), (GIVE, 2, 19), (GIVE, 3, 19), (GIVE, 2, 12),
-    (COMBINE, 0, 11), (COMBINE, 0, 12), (COMBINE, 1, 12), (WGRAD, 1, 1), (GIVE, 0, 4),
-    (GIVE, 0, 5), (GIVE, 1, 4), (GIVE, 3, 12), (COMBINE, 0, 7), (COMBINE, 1, 8), (COMBINE, 1, 9),
-    (WGRAD, 1, 0), (GIVE, 3, 14), (COMBINE, 0, 9), (COMBINE, 1, 11), (COMBINE, 1, 6),
-    (COMBINE, 1, 7), (SUMMED, 1, 0), (SUMMED, 1, 1), (SUMMED, 1, 2), (SUMMED, 1, 3), (BACK, 0),
-    (GIVE, 1, 5), (GIVE, 2, 13), (GIVE, 2, 14), (GIVE, 3, 13), (GIVE, 1, 16), (COMBINE, 0, 3),
-    (COMBINE, 0, 4), (COMBINE, 0, 6), (COMBINE, 0, 8), (GIVE, 2, 15), (GIVE, 3, 15),
-    (COMBINE, 1, 4), (BACK, 1), (GIVE, 2, 16), (GIVE, 2, 17), (GIVE, 3, 16), (GIVE, 3, 17),
-    (COMBINE, 3, 11), (BACK, 2), (GIVE, 3, 5), (GIVE, 0, 6), (GIVE, 1, 6), (GIVE, 1, 7),
-    (COMBINE, 2, 11), (COMBINE, 2, 12), (COMBINE, 2, 6), (COMBINE, 3, 12), (START, 2, 0),
-    (BACK, 3), (GIVE, 2, 4), (GIVE, 2, 5), (GIVE, 3, 4), (GIVE, 0, 7), (COMBINE, 0, 5),
-    (COMBINE, 3, 6), (COMBINE, 3, 8), (START, 2, 1), (COMBINE, 4, 0), (COMBINE, 5, 0), (LATE,),
-    (COMBINE, 2, 7), (COMBINE, 2, 8), (COMBINE, 3, 7), (START, 2, 2), (GIVE, 0, 10),
-    (COMBINE, 1, 3), (GIVE, 0, 9), (GIVE, 0, 8), (GIVE, 0, 11), (COMBINE, 1, 5), (COMBINE, 2, 9),
-    (COMBINE, 3, 9), (GIVE, 1, 9), (START, 2, 3), (COMBINE, 3, 3), (GIVE, 1, 8), (COMBINE, 2, 3),
-    (COMBINE, 2, 4), (COMBINE, 3, 4), (MIDDLE, 2, 0, -1), (MIDDLE, 2, 0, 1), (GIVE, 1, 10),
-    (GIVE, 1, 11), (GIVE, 3, 7), (GIVE, 2, 7), (GIVE, 2, 6), (GIVE, 3, 6), (MIDDLE, 2, 1, -1),
-    (MIDDLE, 2, 1, 1), (MIDDLE, 2, 2, -1), (MIDDLE, 2, 2, 1), (GIVE, 3, 9), (GIVE, 2, 9),
-    (GIVE, 2, 8), (GIVE, 3, 8), (COMBINE, 3, 5), (COMBINE, 2, 5), (MIDDLE, 2, 3, -1),
-    (MIDDLE, 2, 3, 1), (COMBINE, 0, 1), (GIVE, 2, 10), (GIVE, 3, 10), (GIVE, 3, 11),
-    (GIVE, 2, 11), (COMBINE, 0, 2), (SUMMED, 2, 0), (GIVE, 0, 3), (GIVE, 0, 1), (GIVE, 0, 0),
-    (GIVE, 0, 2), (COMBINE, 1, 1), (COMBINE, 1, 2), (SUMMED, 2, 1), (GIVE, 1, 1), (GIVE, 1, 3),
-    (GIVE, 1, 2), (GIVE, 1, 0), (SUMMED, 2, 2), (GIVE, 2, 3), (GIVE, 3, 3), (GIVE, 3, 2),
-    (GIVE, 2, 2), (COMBINE, 2, 1), (COMBINE, 3, 1), (COMBINE, 2, 2), (COMBINE, 3, 2),
-    (SUMMED, 2, 3), (EARLY,), (GIVE, 2, 0), (GIVE, 2, 1), (GIVE, 3, 0), (GIVE, 3, 1),
-    (COMBINE, 0, 0), (COMBINE, 1, 0), (COMBINE, 2, 0), (COMBINE, 3, 0),
+    (GIVE, 4, 14), (GIVE, 4, 15), (NEAR, 5, 1), (NEAR, 5, -1), (COMBINE, 5, 11), (GIVE, 5, 5),
+    (COMBINE, 5, 12), (GIVE, 5, 4), (FAR, 4), (FULL, 4), (DGRAD, 2), (GIVE, 5, 12), (GIVE, 5, 13),
+    (GIVE, 5, 14), (GIVE, 5, 15), (NEAR, 6, 1), (NEAR, 6, -1), (COMBINE, 4, 9), (COMBINE, 4, 11),
+    (GIVE, 4, 5), (COMBINE, 4, 12), (GIVE, 4, 4), (HIDDEN, 3), (GIVE, 4, 16), (GIVE, 4, 17),
+    (FAR, 5), (START, 1, 0), (COMBINE, 5, 5), (START, 1, 1), (GIVE, 5, 10), (GIVE, 5, 11),
+    (START, 1, 2), (START, 1, 3), (GIVE, 4, 8), (FULL, 5), (DGRAD, 3), (GIVE, 5, 16),
+    (GIVE, 5, 17), (COMBINE, 4, 6), (GIVE, 4, 7), (COMBINE, 4, 7), (COMBINE, 4, 8), (HIDDEN, 2),
+    (GIVE, 4, 6), (GIVE, 4, 9), (COMBINE, 5, 6), (GIVE, 5, 7), (FAR, 6), (COMBINE, 5, 7),
+    (GIVE, 5, 6), (COMBINE, 5, 8), (GIVE, 5, 9), (COMBINE, 5, 9), (GIVE, 5, 8), (COMBINE, 4, 5),
+    (MIDDLE, 1, 0, 1), (MIDDLE, 1, 0, -1), (MIDDLE, 1, 1, 1), (FULL, 6), (DGRAD, 4),
+    (GIVE, 4, 10), (GIVE, 4, 11), (COMBINE, 4, 3), (COMBINE, 4, 4), (HIDDEN, 0), (GIVE, 4, 3),
+    (GIVE, 4, 2), (COMBINE, 5, 3), (GIVE, 5, 3), (COMBINE, 5, 4), (GIVE, 5, 2), (HIDDEN, 1),
+    (DERIVE,), (WGRAD, 0, 3), (GIVE, 0, 12), (GIVE, 0, 13), (GIVE, 0, 18), (GIVE, 0, 19),
+    (GIVE, 1, 14), (GIVE, 1, 15), (COMBINE, 5, 1), (WGRAD, 0, 2), (GIVE, 0, 14), (GIVE, 0, 15),
+    (GIVE, 1, 12), (GIVE, 1, 13), (WGRAD, 0, 1), (GIVE, 1, 18), (GIVE, 1, 19), (GIVE, 0, 16),
+    (GIVE, 0, 17), (COMBINE, 5, 2), (WGRAD, 0, 0), (GIVE, 1, 16), (GIVE, 1, 17), (COMBINE, 4, 1),
+    (GIVE, 4, 1), (COMBINE, 4, 2), (GIVE, 4, 0), (WGRAD, 1, 3), (GIVE, 2, 12), (GIVE, 2, 13),
+    (WGRAD, 1, 2), (GIVE, 2, 14), (GIVE, 2, 15), (GIVE, 2, 18), (GIVE, 2, 19), (COMBINE, 0, 11),
+    (COMBINE, 0, 12), (WGRAD, 1, 1), (GIVE, 3, 12), (GIVE, 3, 13), (GIVE, 3, 18), (GIVE, 3, 19),
+    (COMBINE, 0, 6), (COMBINE, 0, 7), (COMBINE, 1, 8), (COMBINE, 1, 9), (BACK, 0), (GIVE, 3, 14),
+    (GIVE, 3, 15), (GIVE, 0, 5), (GIVE, 0, 4), (COMBINE, 0, 8), (COMBINE, 0, 9), (COMBINE, 1, 6),
+    (COMBINE, 1, 7), (BACK, 1), (GIVE, 2, 16), (GIVE, 2, 17), (GIVE, 3, 16), (GIVE, 3, 17),
+    (GIVE, 0, 7), (GIVE, 0, 6), (COMBINE, 0, 3), (COMBINE, 0, 4), (COMBINE, 1, 3),
+    (COMBINE, 1, 4), (COMBINE, 1, 11), (COMBINE, 1, 12), (BACK, 2), (GIVE, 1, 7), (GIVE, 1, 6),
+    (COMBINE, 2, 6), (COMBINE, 2, 7), (START, 2, 0), (BACK, 3), (GIVE, 1, 5), (GIVE, 1, 4),
+    (GIVE, 1, 9), (GIVE, 1, 8), (COMBINE, 2, 8), (COMBINE, 2, 9), (COMBINE, 2, 11),
+    (COMBINE, 2, 12), (COMBINE, 3, 6), (COMBINE, 3, 7), (COMBINE, 3, 11), (COMBINE, 3, 12),
+    (START, 2, 1), (WGRAD, 1, 0), (GIVE, 3, 5), (GIVE, 3, 4), (COMBINE, 3, 8), (COMBINE, 3, 9),
+    (START, 2, 2), (MIDDLE, 1, 1, -1), (MIDDLE, 1, 2, 1), (MIDDLE, 1, 2, -1), (MIDDLE, 1, 3, 1),
+    (MIDDLE, 1, 3, -1), (SUMMED, 1, 0), (COMBINE, 4, 0), (GIVE, 2, 5), (COMBINE, 2, 3),
+    (GIVE, 2, 4), (COMBINE, 2, 4), (COMBINE, 0, 5), (START, 2, 3), (GIVE, 0, 9), (GIVE, 0, 8),
+    (COMBINE, 3, 3), (COMBINE, 3, 4), (MIDDLE, 2, 0, 1), (MIDDLE, 2, 0, -1), (GIVE, 0, 10),
+    (GIVE, 0, 11), (GIVE, 2, 7), (GIVE, 2, 6), (GIVE, 3, 7), (MIDDLE, 2, 1, 1), (GIVE, 3, 6),
+    (MIDDLE, 2, 1, -1), (COMBINE, 1, 5), (MIDDLE, 2, 2, 1), (MIDDLE, 2, 2, -1), (GIVE, 1, 10),
+    (GIVE, 1, 11), (GIVE, 3, 9), (GIVE, 3, 8), (GIVE, 2, 9), (GIVE, 2, 8), (COMBINE, 3, 5),
+    (SUMMED, 1, 1), (GIVE, 0, 3), (GIVE, 0, 2), (COMBINE, 2, 5), (GIVE, 3, 10), (GIVE, 3, 11),
+    (SUMMED, 1, 2), (COMBINE, 0, 1), (COMBINE, 0, 2), (GIVE, 0, 1), (GIVE, 0, 0), (GIVE, 2, 10),
+    (GIVE, 2, 11), (MIDDLE, 2, 3, 1), (GIVE, 2, 3), (GIVE, 2, 2), (SUMMED, 1, 3), (LATE,),
+    (GIVE, 1, 3), (GIVE, 1, 2), (COMBINE, 1, 1), (COMBINE, 1, 2), (MIDDLE, 2, 3, -1),
+    (GIVE, 1, 1), (GIVE, 1, 0), (GIVE, 3, 3), (GIVE, 3, 2), (SUMMED, 2, 0), (GIVE, 5, 1),
+    (COMBINE, 3, 1), (GIVE, 5, 0), (COMBINE, 3, 2), (SUMMED, 2, 1), (COMBINE, 2, 1), (GIVE, 2, 1),
+    (COMBINE, 2, 2), (GIVE, 2, 0), (GIVE, 3, 1), (COMBINE, 0, 0), (GIVE, 3, 0), (SUMMED, 2, 2),
+    (SUMMED, 2, 3), (EARLY,), (COMBINE, 1, 0), (COMBINE, 5, 0), (COMBINE, 2, 0), (COMBINE, 3, 0),
 ]
 
 

time: 103 us -> 103 us (level)
  no operation moved by 1% of the time
where the time goes in v4:
time: 103 us; the launch traced here: 102 us
  Pallas kernels  101 us (98%)
    pallas_call x1, Pallas kernels, per_device(): pl.pallas_call(kernel, name='half_step', out_shape=(vmem((64, 2048), BF),...  100 us

profile of v4, /device:TPU:0, one launch (start us, length us, event | category | flops | bytes accessed | tf_op | source)
XLA Modules:
  0.0 101.9 jit_solution(5865910157850061653)
XLA Ops:
  0.6 100.0 %half_step.1 = (bf16[64,2048]{1,0:T(8,128)(2,1)S(1)}, bf16[64,2048]{1,0:T(8,128)(2,1)S(1)}, f32[128,512]{1,0:T(8,128)S(1)}, f32[128,512]{1,0:T(8,128)S(1)}, f32[128,512]{1,0:T(8,128)S(1)}) custom-call(bf16[64,2048]{1,0:T(8,128)(2,1)} %late_in.1, bf16[64,2048]{1,0:T(8,128)(2,1)} %early_in.1, bf16[64,2048]{1,0:T(8,128)(2,1)} %early_grad.1, f32[1,2048]{1,0:T(1,128)} %bitcast.2, ...), custom_call_target="tpu_custom_call" | custom-call | tf_op jit(solution)/shard_map/half_step/pallas_call | solution.py:605
  100.7 1.1 %hand_over.1 = (bf16[64,2048]{1,0:T(8,128)(2,1)}, bf16[64,2048]{1,0:T(8,128)(2,1)}, f32[128,512]{1,0:T(8,128)}, f32[128,512]{1,0:T(8,128)}, f32[128,512]{1,0:T(8,128)}) custom-call(bf16[64,2048]{1,0:T(8,128)(2,1)S(1)} %get-tuple-element.10.refs_0_, bf16[64,2048]{1,0:T(8,128)(2,1)S(1)} %get-tuple-element.11.refs_1_, ...), custom_call_target="tpu_custom_call" | custom-call | tf_op jit(solution)/shard_map/hand_over/pallas_call | solution.py:657
